TPU v7x, 32 devices: a whole 2x2x4 slice. The times are simulated.
32 devices in a mesh: ep: 8 (over z, core), tp: 4 (over y, x).
Axes of the slice: x: 2, y: 2, z: 4, core: 2. Of those that a mesh axis runs over, the one named last changes fastest.
Arguments:
- tokens: bfloat16 [256, 4096], P('ep'), may hold values from -6 to 6
- recur_state: float32 [256, 4096], P('ep', 'tp'), may hold values from -6 to 6
- conv_state: bfloat16 [256, 3, 4096], P('ep', None, 'tp'), may hold values from -6 to 6
- mix_gain: float32 [4096], replicated, may hold values from 0.1 to 1.9
- in_weight: bfloat16 [4096, 4096], P('ep', 'tp'), may hold values from -0.09375 to 0.09375
- gate_weight: bfloat16 [4096, 4096], P('ep', 'tp'), may hold values from -0.09375 to 0.09375
- conv_taps: float32 [4, 4096], P(None, 'tp'), may hold values from -3 to 3
- recur_gate_blocks: bfloat16 [64, 64, 64], P('tp'), may hold values from -0.75 to 0.75
- input_gate_blocks: bfloat16 [64, 64, 64], P('tp'), may hold values from -0.75 to 0.75
- decay_rate: float32 [4096], P('tp'), may hold values from 0.01 to 0.4
- out_weight: bfloat16 [4096, 4096], P('tp', 'ep'), may hold values from -0.09375 to 0.09375
- ffn_gain: float32 [4096], replicated, may hold values from 0.1 to 1.9
- router_weight: bfloat16 [4096, 8], replicated, may hold values from -0.09375 to 0.09375
- routes: int32 [256, 2], P('ep'), may hold values from 0 to 7, as said below
- expert_gate: bfloat16 [8, 4096, 2048], P('ep', None, 'tp'), may hold values from -0.09375 to 0.09375
- expert_up: bfloat16 [8, 4096, 2048], P('ep', None, 'tp'), may hold values from -0.09375 to 0.09375
- expert_down: bfloat16 [8, 2048, 4096], P('ep', 'tp'), may hold values from -0.125 to 0.125
- dense_gate: bfloat16 [4096, 2048], P('ep', 'tp'), may hold values from -0.09375 to 0.09375
- dense_up: bfloat16 [4096, 2048], P('ep', 'tp'), may hold values from -0.09375 to 0.09375
- dense_down: bfloat16 [2048, 4096], P('tp', 'ep'), may hold values from -0.125 to 0.125
- branch_gate: bfloat16 [4096], replicated, may hold values from -0.09375 to 0.09375
Outputs:
- layer_out: bfloat16 [256, 4096], P('ep')
- new_state: float32 [256, 4096], P('ep', 'tp')
- new_conv_state: bfloat16 [256, 3, 4096], P('ep', None, 'tp')
Inputs may be any that keep to these rules, and one draw needn't show every extreme that they name: `routes`: A row names two different experts of one group: both have the same e // 4. In the rows of one index of ep no expert is named more than 16 times, and in every draw some expert is named exactly 16 times by the rows of every index of ep.
All inputs are finite; a program needn't handle non-finite values.
Results may differ from a plain program's by a relative error of at most 0.023.
Values may be sent and summed in bfloat16 or wider, within the bound.
A program may use at most 64 MiB of HBM per device.

v0:
```python
import functools

import jax
import jax.numpy as jnp
from jax import lax
from jax.experimental import pallas as pl
from jax.experimental.pallas import tpu as pltpu
from jax.sharding import PartitionSpec as P

TOP_K = 2
LANES = 128
F32 = jnp.float32
BF16 = jnp.bfloat16


epsilon = 1e-06
decay_scale = 8.0


def rms_scale(rows, gain):
    values = rows.astype(jnp.float32)
    inverse = lax.rsqrt(jnp.mean(values * values, axis=-1, keepdims=True) + epsilon)
    return (values * inverse * gain).astype(jnp.bfloat16)


def on_device(
    tokens,
    recur_state,
    conv_state,
    mix_gain,
    in_weight,
    gate_weight,
    conv_taps,
    recur_gate_blocks,
    input_gate_blocks,
    decay_rate,
    out_weight,
    ffn_gain,
    router_weight,
    routes,
    expert_gate,
    expert_up,
    expert_down,
    dense_gate,
    dense_up,
    dense_down,
    branch_gate,
):
    batch_rows, width = tokens.shape
    channels = in_weight.shape[1]
    normed = rms_scale(tokens, mix_gain)
    arrived = lax.all_to_all(normed, "ep", split_axis=1, concat_axis=0, tiled=True)
    joined = jnp.concatenate([in_weight, gate_weight], axis=1)
    summed = lax.psum_scatter(
        jnp.dot(arrived, joined, preferred_element_type=jnp.float32).astype(jnp.bfloat16),
        "ep",
        scatter_dimension=0,
        tiled=True,
    ).astype(jnp.float32)
    x_sum, gate_sum = (summed[:, :channels], summed[:, channels:])
    x_branch = x_sum.astype(jnp.bfloat16)
    gate_branch = gate_sum.astype(jnp.bfloat16)
    window = jnp.concatenate([conv_state, x_branch[:, None, :]], axis=1)
    conv_out = jnp.sum(window.astype(jnp.float32) * conv_taps[None], axis=1).astype(jnp.bfloat16)
    new_conv_state = window[:, 1:, :]
    blocks = conv_out.reshape(batch_rows, recur_gate_blocks.shape[0], recur_gate_blocks.shape[1])
    recur_gate = jax.nn.sigmoid(
        jnp.einsum(
            "bhi,hij->bhj", blocks, recur_gate_blocks, preferred_element_type=jnp.float32
        ).reshape(batch_rows, channels)
    )
    input_gate = jax.nn.sigmoid(
        jnp.einsum(
            "bhi,hij->bhj", blocks, input_gate_blocks, preferred_element_type=jnp.float32
        ).reshape(batch_rows, channels)
    )
    log_decay = -decay_scale * recur_gate * decay_rate
    new_state = jnp.exp(log_decay) * recur_state + jnp.sqrt(
        -jnp.expm1(2.0 * log_decay)
    ) * input_gate * conv_out.astype(jnp.float32)
    mixer_rows = (new_state * jax.nn.gelu(gate_branch.astype(jnp.float32))).astype(jnp.bfloat16)
    mixer_part = jnp.dot(
        mixer_rows,
        lax.all_gather(out_weight, "ep", axis=1, tiled=True),
        preferred_element_type=jnp.float32,
    )
    resid = (
        tokens.astype(jnp.float32)
        + lax.psum(mixer_part.astype(jnp.bfloat16), "tp").astype(jnp.float32)
    ).astype(jnp.bfloat16)
    normed_ffn = rms_scale(resid, ffn_gain)
    router_logits = jnp.dot(normed_ffn, router_weight, preferred_element_type=jnp.float32)
    experts = router_logits.shape[1]
    expert_ids = lax.broadcasted_iota(jnp.int32, (batch_rows, TOP_K, experts), 2)
    picked = jnp.sum(
        jnp.where(routes[:, :, None] == expert_ids, router_logits[:, None, :], 0.0), axis=2
    )
    route_weight = jax.nn.sigmoid(picked - picked[:, ::-1]).astype(jnp.bfloat16)
    capacity = 2 * batch_rows * TOP_K // experts
    flat_ids = routes.reshape(batch_rows * TOP_K)
    onehot = (
        flat_ids[:, None] == lax.broadcasted_iota(jnp.int32, (batch_rows * TOP_K, experts), 1)
    ).astype(jnp.int32)
    rank = jnp.sum((jnp.cumsum(onehot, axis=0) - onehot) * onehot, axis=1)
    slot_of = (flat_ids * capacity + rank).reshape(batch_rows, TOP_K)
    slot_rows = lax.broadcasted_iota(jnp.int32, (experts * capacity, batch_rows), 0)
    slot_cols = lax.broadcasted_iota(jnp.int32, (batch_rows, experts * capacity), 1)
    dispatch = jnp.zeros((experts * capacity, batch_rows), jnp.bfloat16)
    combine = jnp.zeros((batch_rows, experts * capacity), jnp.bfloat16)
    for pick in range(TOP_K):
        dispatch = dispatch + (slot_rows == slot_of[None, :, pick]).astype(jnp.bfloat16)
        combine = combine + jnp.where(
            slot_cols == slot_of[:, pick : pick + 1],
            route_weight[:, pick : pick + 1],
            jnp.zeros((), jnp.bfloat16),
        )
    outgoing = (
        jnp.dot(dispatch, normed_ffn, preferred_element_type=jnp.float32)
        .astype(jnp.bfloat16)
        .reshape(experts, capacity, width)
    )
    gate_local = expert_gate[0]
    up_local = expert_up[0]
    down_local = expert_down[0]
    arrived_rows = lax.all_to_all(outgoing, "ep", split_axis=0, concat_axis=0, tiled=True)
    sources, items, features = arrived_rows.shape
    rows = arrived_rows.reshape(sources * items, features)
    first = jnp.dot(rows, gate_local, preferred_element_type=jnp.float32)
    second = jnp.dot(rows, up_local, preferred_element_type=jnp.float32)
    act = (jax.nn.silu(first) * second).astype(jnp.bfloat16)
    partial_value = jnp.dot(act, down_local, preferred_element_type=jnp.float32)
    total = lax.psum(partial_value.astype(jnp.bfloat16), "tp")
    returned = lax.all_to_all(
        total.reshape(sources, items, total.shape[1]), "ep", split_axis=0, concat_axis=0, tiled=True
    )
    moe = jnp.dot(
        combine,
        returned.reshape(experts * capacity, returned.shape[2]),
        preferred_element_type=jnp.float32,
    )
    dense_arrived = lax.all_to_all(normed_ffn, "ep", split_axis=1, concat_axis=0, tiled=True)
    dense_joined = jnp.concatenate([dense_gate, dense_up], axis=1)
    dense_summed = lax.psum_scatter(
        jnp.dot(dense_arrived, dense_joined, preferred_element_type=jnp.float32).astype(
            jnp.bfloat16
        ),
        "ep",
        scatter_dimension=0,
        tiled=True,
    ).astype(jnp.float32)
    dense_first = dense_summed[:, : dense_gate.shape[1]]
    dense_second = dense_summed[:, dense_gate.shape[1] :]
    dense_act = (jax.nn.silu(dense_first) * dense_second).astype(jnp.bfloat16)
    dense_part = jnp.dot(
        dense_act,
        lax.all_gather(dense_down, "ep", axis=1, tiled=True),
        preferred_element_type=jnp.float32,
    )
    branch_weight = jax.nn.sigmoid(
        jnp.dot(normed_ffn, branch_gate, preferred_element_type=jnp.float32)
    )
    dense_sum = lax.psum(dense_part.astype(jnp.bfloat16), "tp").astype(jnp.float32)
    layer_out = (resid.astype(jnp.float32) + moe + branch_weight[:, None] * dense_sum).astype(
        jnp.bfloat16
    )
    return (layer_out, new_state, new_conv_state)


def rcopy(src, dst, send, recv, ep, tp):
    return pltpu.make_async_remote_copy(
        src_ref=src,
        dst_ref=dst,
        send_sem=send,
        recv_sem=recv,
        device_id={"ep": ep, "tp": tp},
        device_id_type=pl.DeviceIdType.MESH,
    )


def greet(peers):
    barrier = pltpu.get_barrier_semaphore()
    for ep, tp in peers:
        pl.semaphore_signal(
            barrier, inc=1, device_id={"ep": ep, "tp": tp}, device_id_type=pl.DeviceIdType.MESH
        )
    pl.semaphore_wait(barrier, len(peers))


def dot(left, right):
    return jnp.dot(left, right, preferred_element_type=F32)


def split_sum(me, tp, zs, half, psend, precv, keep, rsend, rrecv, s2, r2, s3, r3, part, between):
    z, c = me // 2, me % 2
    mate = 2 * z + 1 - c
    sends = []
    for zz in range(zs):
        psend[zz] = part(zz, 1 - c)
        cp = rcopy(psend.at[zz], precv.at[zz], s2.at[zz], r2.at[zz], mate, tp)
        cp.start()
        sends.append(cp)
    for zz in range(zs):
        keep[zz] = part(zz, c).astype(F32)
    between()
    for dz in range(1, zs):
        zz = lax.rem(z + dz, zs)
        rcopy(psend.at[zz], precv.at[zz], s2.at[zz], r2.at[zz], mate, tp).wait_recv()
        rsend[zz] = (keep[zz] + precv[zz].astype(F32)).astype(BF16)
        cp = rcopy(rsend.at[zz], rrecv.at[z], s3.at[dz], r3.at[dz], 2 * zz + c, tp)
        cp.start()
        sends.append(cp)
    rcopy(psend.at[z], precv.at[z], s2.at[z], r2.at[z], mate, tp).wait_recv()

    def finish():
        total = keep[z] + precv[z].astype(F32)
        for dz in range(1, zs):
            frm = lax.rem(z - dz + zs, zs)
            rcopy(rrecv.at[frm], rrecv.at[frm], s3.at[dz], r3.at[dz], mate, tp).wait_recv()
            total += rrecv[frm].astype(F32)
        return total

    return sends, finish


def project_kernel(
    n, tokens, gain, iw_hbm, gw_hbm, out, toks, iw, gw, lw, narr, psend, precv, keep, rsend, rrecv, s1, r1, s2, r2, s3, r3
):
    me, tp = lax.axis_index("ep"), lax.axis_index("tp")
    zs = n // 2
    q, ch = iw.shape
    g = toks.shape[2]
    loads = [
        pltpu.make_async_copy(iw_hbm, iw, lw.at[0]),
        pltpu.make_async_copy(gw_hbm, gw, lw.at[1]),
    ]
    for cp in loads:
        cp.start()
    greet([(lax.rem(me + d, n), tp) for d in range(1, n)])

    def columns(e):
        return pl.ds(pl.multiple_of(e * q, LANES), q)

    sends = []
    for d in range(1, n):
        to = lax.rem(me + d, n)
        cp = rcopy(tokens.at[:, columns(to)], narr.at[me], s1.at[d], r1.at[d], to, tp)
        cp.start()
        sends.append(cp)
    narr[me] = tokens[:, columns(me)]
    values = tokens[...].astype(F32)
    inverse = lax.rsqrt(jnp.mean(values * values, axis=-1, keepdims=True) + epsilon)
    for cp in loads:
        cp.wait()
    for d in range(1, n):
        frm = lax.rem(me - d + n, n)
        rcopy(narr.at[frm], narr.at[frm], s1.at[d], r1.at[d], frm, tp).wait_recv()

    def part(zz, core):
        rows = (narr[2 * zz + core].astype(F32) * gain[me]).astype(BF16)
        return jnp.concatenate([dot(rows, iw[...]), dot(rows, gw[...])], axis=1).astype(psend.dtype)

    more, finish = split_sum(
        me, tp, zs, None, psend, precv, keep, rsend, rrecv, s2, r2, s3, r3, part, lambda: None
    )
    toks[...] = narr[:, :, pl.ds(pl.multiple_of(tp * g, LANES), g)]
    out[...] = (finish() * inverse).astype(BF16)
    for cp in sends + more:
        cp.wait_send()


def project(n, m, tokens, gain, iw, gw):
    rows, width = tokens.shape
    q, ch = iw.shape
    zs = n // 2
    vm = pl.BlockSpec(memory_space=pltpu.VMEM)
    dma = pltpu.SemaphoreType.DMA
    return pl.pallas_call(
        functools.partial(project_kernel, n),
        out_shape=(
            jax.ShapeDtypeStruct((rows, 2 * ch), BF16),
            jax.ShapeDtypeStruct((n, rows, q // m), BF16),
        ),
        in_specs=[vm] * 2 + [pl.BlockSpec(memory_space=pl.ANY)] * 2,
        out_specs=(vm, vm),
        scratch_shapes=[
            pltpu.VMEM((q, ch), BF16),
            pltpu.VMEM((q, ch), BF16),
            dma((2,)),
            pltpu.VMEM((n, rows, q), BF16),
            pltpu.VMEM((zs, rows, 2 * ch), BF16),
            pltpu.VMEM((zs, rows, 2 * ch), BF16),
            pltpu.VMEM((zs, rows, 2 * ch), F32),
            pltpu.VMEM((zs, rows, 2 * ch), BF16),
            pltpu.VMEM((zs, rows, 2 * ch), BF16),
            dma((n,)),
            dma((n,)),
            dma((zs,)),
            dma((zs,)),
            dma((zs,)),
            dma((zs,)),
        ],
        compiler_params=pltpu.CompilerParams(
            collective_id=0, has_side_effects=True, vmem_limit_bytes=60 * 1024 * 1024
        ),
        name="project",
    )(tokens, gain, iw, gw)


def layer_kernel(
    n, m, experts, mr, toks, gain, mask, rb, bg, ow_hbm, dg_hbm, du_hbm, dd_hbm, eg, eu, ed, out,
    ow, dg, du, dd, lacc, square, bacc, wg, wu, wd, mall, masks, osend, orecv, full, nf, accg, accu, act,
    psend, precv, dkeep, rsend, rrecv, dact, dall,
    ysend, yrecv, keep, xsend, xrecv, zsend, zrecv, fblk, fin,
    lw, ks, kr, as_, ar, bs, br, os_, or_, zs_, zr, xs, xr, ms, mrv,
    s2, r2, s3, r3, cs, cr, es, er, ys, yr, hs, hr, gs, gr, fs, fr,
):
    me, tp = lax.axis_index("ep"), lax.axis_index("tp")
    zs = n // 2
    z, c = me // 2, me % 2
    mate = 2 * z + 1 - c
    rows, width = out.shape
    q = ow.shape[1]
    g = q // m
    peers = [(lax.rem(me + d, n), tp) for d in range(1, n)]
    for d in range(1, m):
        peers += [(me, lax.rem(tp + d, m)), (mate, lax.rem(tp + d, m))]
    small = [
        pltpu.make_async_copy(a, b, lw.at[n + 2 + k])
        for k, (a, b) in enumerate(((ow_hbm, ow), (dg_hbm, dg), (du_hbm, du), (dd_hbm, dd)))
    ]
    for cp in small:
        cp.start()
    loads = [
        pltpu.make_async_copy(eg, wg, lw.at[n]),
        pltpu.make_async_copy(eu, wu, lw.at[n + 1]),
    ] + [
        pltpu.make_async_copy(ed.at[:, pl.ds(i * q, q)], wd.at[i], lw.at[i]) for i in range(n)
    ]
    for cp in loads:
        cp.start()
    greet(peers)
    sends = []

    def send(*args):
        cp = rcopy(*args)
        cp.start()
        sends.append(cp)

    def arrive(buf, sem):
        rcopy(buf, buf, sem, sem, mate, tp).wait_recv()

    def zpeer(dz):
        return lax.rem(z + dz, zs)

    def zfrom(dz):
        return lax.rem(z - dz + zs, zs)

    def tto(dt):
        return lax.rem(tp + dt, m)

    def tfrom(dt):
        return lax.rem(tp - dt + m, m)

    def gather(own, buf, s_a, r_a, s_b, r_b):
        for dz in range(1, zs):
            send(own, buf.at[me], s_a.at[dz], r_a.at[dz], 2 * zpeer(dz) + c, tp)
        send(own, buf.at[me], s_b.at[0], r_b.at[0], mate, tp)
        buf[me] = own[...]
        for dz in range(1, zs):
            slot = 2 * zfrom(dz) + c
            arrive(buf.at[slot], r_a.at[dz])
            send(buf.at[slot], buf.at[slot], s_b.at[dz], r_b.at[dz], mate, tp)

    def gathered(buf, r_b):
        for dz in range(zs):
            arrive(buf.at[2 * zfrom(dz) + 1 - c], r_b.at[dz])

    gather(mr, mall, as_, ar, bs, br)
    for d in range(1, n):
        send(mask, masks.at[me], ks.at[d], kr.at[d], lax.rem(me + d, n), tp)
    masks[me] = mask[...]
    for cp in small:
        cp.wait()
    gathered(mall, br)
    mixed = dot(mall[...].reshape(n * rows, mr.shape[1]), ow[...]).astype(BF16)
    for t in range(m):
        osend[t] = mixed[:, t * g : (t + 1) * g].reshape(n, rows, g)
    for dt in range(1, m):
        send(osend.at[tto(dt)], orecv.at[tp], os_.at[dt], or_.at[dt], me, tto(dt))
    total = toks[...].astype(F32) + osend[tp].astype(F32)
    accg[...] = jnp.zeros_like(accg)
    accu[...] = jnp.zeros_like(accu)
    lacc[...] = jnp.zeros_like(lacc)
    square[...] = jnp.zeros_like(square)
    bacc[...] = jnp.zeros_like(bacc)
    for dt in range(1, m):
        arrive(orecv.at[tfrom(dt)], or_.at[dt])
        total += orecv[tfrom(dt)].astype(F32)
    full[tp, me] = total.astype(BF16)

    def spread(slot, dz):
        for dt in range(1, m):
            k = dz * m + dt
            send(full.at[tp, slot], full.at[tp, slot], xs.at[k], xr.at[k], 2 * z + c, tto(dt))
        k = dz * m
        send(full.at[tp, slot], full.at[tp, slot], ms.at[k], mrv.at[k], mate, tp)

    for dz in range(1, zs):
        send(full.at[tp, me], full.at[tp, me], zs_.at[dz], zr.at[dz], 2 * zpeer(dz) + c, tp)
    spread(me, 0)
    for dz in range(1, zs):
        slot = 2 * zfrom(dz) + c
        arrive(full.at[tp, slot], zr.at[dz])
        spread(slot, dz)
    def relay(dz):
        slot = 2 * zfrom(dz) + c
        for dt in range(1, m):
            k = dz * m + dt
            at = full.at[tfrom(dt), slot]
            arrive(at, xr.at[k])
            send(at, at, ms.at[k], mrv.at[k], mate, tp)

    def expert_in(dz):
        slot = 2 * zfrom(dz) + 1 - c
        for dt in range(m):
            arrive(full.at[tfrom(dt), slot], mrv.at[dz * m + dt])

        @pl.loop(0, 2)
        def _(core):
            e = 2 * zfrom(dz) + core
            for t in range(m):
                at = slice(t * g, (t + 1) * g)
                v = full[t, e].reshape(n * rows, g).astype(F32)
                square[...] += v * v
                scaled = (v * gain[e, :, at]).astype(BF16)
                bacc[...] += scaled.astype(F32) * bg[e, :, at].astype(F32)
                nf[e, :, :, at] = scaled.reshape(n, rows, g)
            x = nf[e].reshape(n * rows, q)
            accg[...] += dot(x, wg[e])
            accu[...] += dot(x, wu[e])
            maps = rb[:, pl.ds(pl.multiple_of(e * q, LANES), q)]
            lacc[...] += lax.dot_general(
                x, maps, (((1,), (1,)), ((), ())), preferred_element_type=F32
            )

    loads[0].wait()
    loads[1].wait()
    relay(0)
    relay(1)
    expert_in(0)

    def dpart(zz, core):
        x = nf[me, 2 * zz + core]
        return jnp.concatenate([dot(x, dg[...]), dot(x, du[...])], axis=1).astype(BF16)

    def between():
        for dz in range(2, zs):
            relay(dz)
        expert_in(1)

    more, finish = split_sum(
        me, tp, zs, None, psend, precv, dkeep, rsend, rrecv, s2, r2, s3, r3, dpart, between
    )
    sends += more
    for dz in range(2, zs):
        expert_in(dz)
    inverse = lax.rsqrt(jnp.sum(square[...], axis=-1, keepdims=True) / width + epsilon)
    gate = accg[...] * inverse
    act[...] = (gate * jax.nn.sigmoid(gate) * (accu[...] * inverse)).astype(BF16)
    h = dg.shape[1]
    square[:, 0:1] = inverse
    both = finish() * square[pl.ds(pl.multiple_of(me * rows, rows), rows), 0:1]
    first = both[:, :h]
    dact[...] = (first * jax.nn.sigmoid(first) * both[:, h:]).astype(BF16)
    for dz in range(1, zs):
        send(dact, dall.at[me], cs.at[dz], cr.at[dz], 2 * zpeer(dz) + c, tp)
    send(dact, dall.at[me], es.at[0], er.at[0], mate, tp)
    dall[me] = dact[...]

    logits = lacc[...] * inverse
    for d in range(1, n):
        arrive(masks.at[lax.rem(me - d + n, n)], kr.at[d])
    chosen = masks[...].reshape(n * rows, LANES)[:, :experts].astype(F32)
    named = logits * chosen
    other = jnp.sum(named, axis=-1, keepdims=True) - named
    weight = (jax.nn.sigmoid(logits - other) * chosen).astype(BF16).astype(F32)
    lane = lax.broadcasted_iota(jnp.int32, (n * rows, experts), 1)
    weight = jnp.sum(jnp.where(lane == me, weight, 0.0), axis=-1, keepdims=True)
    branch = jax.nn.sigmoid(jnp.sum(bacc[...], axis=-1, keepdims=True) * inverse)

    for cp in loads[2:]:
        cp.wait()
    order = [lax.rem(z + 1 + i, m) for i in range(m)]
    for i in range(m):
        y = dot(act[...], wd[2 * order[i] + 1 - c]) * weight
        ysend[i] = y.astype(BF16)
        send(ysend.at[i], yrecv.at[i], ys.at[i], yr.at[i], mate, tp)
    for i in range(m):
        keep[i] = dot(act[...], wd[2 * order[i] + c]) * weight
    for dz in range(1, zs):
        slot = 2 * zfrom(dz) + c
        arrive(dall.at[slot], cr.at[dz])
        send(dall.at[slot], dall.at[slot], es.at[dz], er.at[dz], mate, tp)

    def forward(i):
        arrive(yrecv.at[i], yr.at[i])
        keep[i] = keep[i] + yrecv[i].astype(F32)

        @pl.when(order[i] != tp)
        def _():
            dt = lax.rem(order[i] - tp + m, m)
            xsend[i] = keep[i].astype(BF16)
            rcopy(
                xsend.at[i], xrecv.at[dt], hs.at[dt], hr.at[dt], me, order[i]
            ).start()

    for i in range(m - 1):
        forward(i)
    for dz in range(zs):
        arrive(dall.at[2 * zfrom(dz) + 1 - c], er.at[dz])
    keep[m - 1] = keep[m - 1] + dot(dall[...].reshape(n * rows, h), dd[...]) * branch
    forward(m - 1)

    mine = lax.rem(tp - z - 1 + 2 * m, m)
    total = keep[mine]
    for dt in range(1, m):
        arrive(xrecv.at[dt], hr.at[dt])
        total += xrecv[dt].astype(F32)
    keep[mine] = total
    for zz in range(zs):
        zsend[zz] = total[2 * zz * rows : 2 * (zz + 1) * rows].astype(BF16)
    for dz in range(1, zs):
        send(zsend.at[zpeer(dz)], zrecv.at[z], gs.at[dz], gr.at[dz], 2 * zpeer(dz) + c, tp)
    at = pl.multiple_of(2 * z * rows, rows)
    total = keep[mine, pl.ds(at, 2 * rows), :]
    for dz in range(1, zs):
        arrive(zrecv.at[zfrom(dz)], gr.at[dz])
        total += zrecv[zfrom(dz)].astype(F32)
    chunk = 2 * tp + c
    for core in range(2):
        resid = jnp.concatenate([full[t, chunk, 2 * z + core] for t in range(m)], axis=1)
        fblk[core] = (resid.astype(F32) + total[core * rows : (core + 1) * rows]).astype(BF16)
    for dc in range(2):
        for dt in range(m):
            if dc or dt:
                core = lax.rem(c + dc, 2)
                k = dc * m + dt
                send(fblk.at[core], fin.at[chunk], fs.at[k], fr.at[k], 2 * z + core, tto(dt))
    fin[chunk] = fblk[c]
    for dc in range(2):
        for dt in range(m):
            if dc or dt:
                k = dc * m + dt
                arrive(fin.at[2 * tfrom(dt) + lax.rem(c + dc, 2)], fr.at[k])
    for e in range(n):
        out[:, e * q : (e + 1) * q] = fin[e]
    for cp in sends:
        cp.wait_send()
    for dt in range(1, m):
        rcopy(xrecv.at[dt], xrecv.at[dt], hs.at[dt], hr.at[dt], mate, tp).wait_send()


def rest(n, m, experts, mr, toks, gain, mask, rb, bg, ow, dg, du, dd, eg, eu, ed):
    rows, width = mr.shape[0], ow.shape[1] * n
    ch, q = ow.shape
    h, f = dg.shape[1], ed.shape[0]
    g, zs, b = q // m, n // 2, n * rows
    vm = pl.BlockSpec(memory_space=pltpu.VMEM)
    hbm = pl.BlockSpec(memory_space=pl.ANY)
    v = pltpu.VMEM

    def pairs(*counts):
        return [pltpu.SemaphoreType.DMA((k,)) for k in counts for _ in range(2)]

    return pl.pallas_call(
        functools.partial(layer_kernel, n, m, experts),
        out_shape=jax.ShapeDtypeStruct((rows, width), BF16),
        in_specs=[vm] * 6 + [hbm] * 7,
        out_specs=vm,
        scratch_shapes=[
            v((ch, q), BF16), v((q, h), BF16), v((q, h), BF16), v((h, q), BF16),
            v((b, experts), F32), v((b, g), F32), v((b, g), F32),
            v((n, q, f), BF16), v((n, q, f), BF16), v((n, f, q), BF16),
            v((n, rows, ch), BF16), v((n, rows, LANES), BF16),
            v((m, n, rows, g), BF16), v((m, n, rows, g), BF16),
            v((m, n, n, rows, g), BF16), v((n, n, rows, q), BF16),
            v((b, f), F32), v((b, f), F32), v((b, f), BF16),
            v((zs, rows, 2 * h), BF16), v((zs, rows, 2 * h), BF16), v((zs, rows, 2 * h), F32),
            v((zs, rows, 2 * h), BF16), v((zs, rows, 2 * h), BF16),
            v((rows, h), BF16), v((n, rows, h), BF16),
            v((m, b, q), BF16), v((m, b, q), BF16), v((m, b, q), F32),
            v((m, b, q), BF16), v((m, b, q), BF16),
            v((zs, 2 * rows, q), BF16), v((zs, 2 * rows, q), BF16),
            v((2, rows, q), BF16), v((n, rows, q), BF16),
            pltpu.SemaphoreType.DMA((n + 6,)),
        ] + pairs(n, zs, zs, m, zs, zs * m, zs * m, zs, zs, zs, zs, m, m, zs, 2 * m),
        compiler_params=pltpu.CompilerParams(
            collective_id=1, has_side_effects=True, vmem_limit_bytes=58 * 1024 * 1024
        ),
        name="rest",
    )(mr, toks, gain, mask, rb, bg, ow, dg, du, dd, eg, eu, ed)


def in_kernels(
    n, m, tokens, recur_state, conv_state, mix_gain, in_weight, gate_weight, conv_taps,
    recur_gate_blocks, input_gate_blocks, decay_rate, out_weight, ffn_gain, router_weight, routes,
    expert_gate, expert_up, expert_down, dense_gate, dense_up, dense_down, branch_gate,
):
    batch_rows, width = tokens.shape
    channels = in_weight.shape[1]
    experts = router_weight.shape[1]
    q = width // n
    lanes = lax.broadcasted_iota(jnp.int32, (batch_rows, LANES), 1)
    mask = ((routes[:, 0:1] == lanes) | (routes[:, 1:2] == lanes)).astype(BF16)
    summed, toks = project(n, m, tokens, mix_gain.reshape(n, 1, q), in_weight, gate_weight)
    x_branch, gate_branch = summed[:, :channels], summed[:, channels:]
    window = jnp.concatenate([conv_state, x_branch[:, None, :]], axis=1)
    conv_out = jnp.sum(window.astype(F32) * conv_taps[None], axis=1).astype(BF16)
    new_conv_state = window[:, 1:, :]
    blocks = conv_out.reshape(batch_rows, recur_gate_blocks.shape[0], recur_gate_blocks.shape[1])

    def gate_of(maps_of):
        return jax.nn.sigmoid(
            jnp.einsum("bhi,hij->bhj", blocks, maps_of, preferred_element_type=F32).reshape(
                batch_rows, channels
            )
        )

    recur_gate = gate_of(recur_gate_blocks)
    input_gate = gate_of(input_gate_blocks)
    log_decay = -decay_scale * recur_gate * decay_rate
    new_state = jnp.exp(log_decay) * recur_state + jnp.sqrt(
        -jnp.expm1(2.0 * log_decay)
    ) * input_gate * conv_out.astype(F32)
    mixer_rows = (new_state * jax.nn.gelu(gate_branch.astype(F32))).astype(BF16)
    f = expert_down.shape[1]
    layer_out = rest(
        n, m, experts, mixer_rows, toks, ffn_gain.reshape(n, 1, q), mask,
        router_weight.T, branch_gate.reshape(n, 1, q), out_weight, dense_gate, dense_up, dense_down,
        expert_gate.reshape(n, q, f), expert_up.reshape(n, q, f), expert_down[0],
    )
    return (layer_out, new_state, new_conv_state)


def solution(mesh):
    in_specs = (
        P("ep", None),
        P("ep", "tp"),
        P("ep", None, "tp"),
        P(),
        P("ep", "tp"),
        P("ep", "tp"),
        P(None, "tp"),
        P("tp", None, None),
        P("tp", None, None),
        P("tp"),
        P("tp", "ep"),
        P(),
        P(),
        P("ep", None),
        P("ep", None, "tp"),
        P("ep", None, "tp"),
        P("ep", "tp", None),
        P("ep", "tp"),
        P("ep", "tp"),
        P("tp", "ep"),
        P(),
    )
    out_specs = (P("ep", None), P("ep", "tp"), P("ep", None, "tp"))
    n, m = mesh.shape["ep"], mesh.shape["tp"]

    def body(*args):
        tokens, router, dense = args[0], args[12], args[17]
        q = tokens.shape[1] // n
        fits = n == 2 * m and n == router.shape[1] < LANES and q % (m * LANES) == 0
        fits = fits and tokens.shape[0] % 16 == 0 and dense.shape[1] % LANES == 0
        if fits:
            return in_kernels(n, m, *args)
        return on_device(*args)

    return jax.shard_map(
        body, mesh=mesh, in_specs=in_specs, out_specs=out_specs, check_vma=False
    )
```

profile of v0, /device:TPU:0, one launch (start us, length us, event | category | flops | bytes accessed | tf_op | source)
XLA Modules:
  0.0 110.8 jit_solution(11902669801563353128)
XLA Ops:
  0.6 0.0 copy-start
  0.6 0.0 copy-start.7
  0.7 0.0 copy-start.5
  0.7 0.0 copy-start.2
  0.7 0.0 copy-start.6
  0.7 0.0 copy-start.4
  0.7 27.4 %project.1 = (bf16[32,2048]{1,0:T(8,128)(2,1)}, bf16[8,32,128]{2,1,0:T(8,128)(2,1)}) custom-call(bf16[32,4096]{1,0:T(8,128)(2,1)} %tokens.1, f32[8,1,512]{2,1,0:T(1,128)} %bitcast.22, bf16[512,1024]{1,0:T(8,128)(2,1)} %iw_hbm.1, bf16[512,1024]{1,0:T(8,128)(2,1)} %gw_hbm.1), custom_call_target="tpu_custom_call" | custom-call | tf_op jit(solution)/shard_map/project/pallas_call | solution.py:277
  28.1 0.0 copy-start.3
  28.1 0.9 slice_bitcast_fusion
  29.0 1.0 multiply_reduce_fusion
  30.0 0.1 convert_element_type.24
  30.1 0.0 copy-done
  30.1 0.2 fusion.7
  30.3 0.2 copy.29
  30.5 0.1 div.13
  30.6 0.0 copy-done.7
  30.6 0.2 fusion.3
  30.9 0.2 copy.31
  31.0 0.1 div.15
  31.2 0.0 copy-done.5
  31.2 0.0 copy-done.2
  31.2 0.0 copy-done.3
  31.2 0.8 fusion.15
  32.0 0.0 copy-done.6
  32.0 0.7 fusion.19.mask
  32.7 0.0 copy-done.4
  32.7 0.6 reshape.45.bg
  33.3 0.0 copy-start.1
  33.3 75.1 %rest.1 = bf16[32,4096]{1,0:T(8,128)(2,1)} custom-call(bf16[32,1024]{1,0:T(8,128)(2,1)} %get-tuple-element.7.mr, bf16[8,32,128]{2,1,0:T(8,128)(2,1)} %get-tuple-element.6.toks, f32[8,1,512]{2,1,0:T(1,128)} %bitcast.23, bf16[32,128]{1,0:T(8,128)(2,1)} %fusion.19.mask, bf16[8,4096]{1,0:T(8,128)(2,1)} %bitcast.21, bf16[8,1,512]{2,1,0:T(2,128)(2,1)} %reshape.45.bg, ...), custom_call_target="tpu_custom_call" | custom-call | tf_op jit(solution)/shard_map/rest/pallas_call | solution.py:575
  108.5 0.0 copy-done.1
  108.5 0.7 fusion.8
  109.2 1.7 %copy.38 = bf16[32,4096]{1,0:T(8,128)(2,1)} copy(bf16[32,4096]{1,0:T(8,128)(2,1)} %rest.1) | data formatting | bytes 524288
  (2 shorter events, 0.0 us)
Async XLA Ops:
  0.6 29.5 %copy-start = (bf16[16,64,64]{2,1,0:T(8,128)(2,1)S(1)}, bf16[16,64,64]{2,1,0:T(8,128)(2,1)}, u32[]{:S(2)}) copy-start(bf16[16,64,64]{2,1,0:T(8,128)(2,1)} %param.28) | copy-start | bytes 393220
  0.6 30.0 %copy-start.7 = (bf16[16,64,64]{2,1,0:T(8,128)(2,1)S(1)}, bf16[16,64,64]{2,1,0:T(8,128)(2,1)}, u32[]{:S(2)}) copy-start(bf16[16,64,64]{2,1,0:T(8,128)(2,1)} %param.29) | copy-start | bytes 393220
  0.7 30.5 %copy-start.5 = (f32[1024]{0:T(1024)S(1)}, f32[1024]{0:T(1024)}, u32[]{:S(2)}) copy-start(f32[1024]{0:T(1024)} %param.30) | copy-start | bytes 12292
  0.7 30.5 %copy-start.2 = (f32[32,1024]{1,0:T(8,128)S(1)}, f32[32,1024]{1,0:T(8,128)}, u32[]{:S(2)}) copy-start(f32[32,1024]{1,0:T(8,128)} %param.22) | copy-start | bytes 393220
  0.7 31.4 %copy-start.6 = (s32[32,2]{0,1:T(2,128)S(1)}, s32[32,2]{0,1:T(2,128)}, u32[]{:S(2)}) copy-start(s32[32,2]{0,1:T(2,128)} %param.34) | copy-start | bytes 772
  0.7 32.0 %copy-start.4 = (bf16[4096]{0:T(1024)(128)(2,1)S(1)}, bf16[4096]{0:T(1024)(128)(2,1)}, u32[]{:S(2)}) copy-start(bf16[4096]{0:T(1024)(128)(2,1)} %param.41) | copy-start | bytes 24580
  28.1 3.1 %copy-start.3 = (bf16[32,2048]{1,0:T(8,128)(2,1)S(1)}, bf16[32,2048]{1,0:T(8,128)(2,1)}, u32[]{:S(2)}) copy-start(bf16[32,2048]{1,0:T(8,128)(2,1)} %get-tuple-element.5) | copy-start | bytes 393220
  33.3 75.1 %copy-start.1 = (bf16[32,3,1024]{2,0,1:T(8,128)(2,1)S(1)}, bf16[32,3,1024]{2,0,1:T(8,128)(2,1)}, u32[]{:S(2)}) copy-start(bf16[32,3,1024]{2,0,1:T(8,128)(2,1)} %param.23) | copy-start | bytes 589828
where the time goes:
time: 111 us
  Pallas kernels  102 us (92%)
  local copies, waits for them, and re-layouts  3.94 us (4%)
  other arithmetic  3.19 us (3%)
    pallas_call x1, Pallas kernels, rest(): pl.pallas_call(functools.partial(layer_kernel, n, m, experts), out_shape=...  75.1 us
    pallas_call x1, Pallas kernels, project(): pl.pallas_call(functools.partial(project_kernel, n), out_shape=(jax.Shape...  27.4 us

commit v1 on v0

v1 whole, which is shorter than its diff:
```python
import functools

import jax
import jax.numpy as jnp
from jax import lax
from jax.experimental import pallas as pl
from jax.experimental.pallas import tpu as pltpu
from jax.sharding import PartitionSpec as P

TOP_K = 2
LANES = 128
F32 = jnp.float32
BF16 = jnp.bfloat16


epsilon = 1e-06
decay_scale = 8.0


def rms_scale(rows, gain):
    values = rows.astype(jnp.float32)
    inverse = lax.rsqrt(jnp.mean(values * values, axis=-1, keepdims=True) + epsilon)
    return (values * inverse * gain).astype(jnp.bfloat16)


def on_device(
    tokens,
    recur_state,
    conv_state,
    mix_gain,
    in_weight,
    gate_weight,
    conv_taps,
    recur_gate_blocks,
    input_gate_blocks,
    decay_rate,
    out_weight,
    ffn_gain,
    router_weight,
    routes,
    expert_gate,
    expert_up,
    expert_down,
    dense_gate,
    dense_up,
    dense_down,
    branch_gate,
):
    batch_rows, width = tokens.shape
    channels = in_weight.shape[1]
    normed = rms_scale(tokens, mix_gain)
    arrived = lax.all_to_all(normed, "ep", split_axis=1, concat_axis=0, tiled=True)
    joined = jnp.concatenate([in_weight, gate_weight], axis=1)
    summed = lax.psum_scatter(
        jnp.dot(arrived, joined, preferred_element_type=jnp.float32).astype(jnp.bfloat16),
        "ep",
        scatter_dimension=0,
        tiled=True,
    ).astype(jnp.float32)
    x_sum, gate_sum = (summed[:, :channels], summed[:, channels:])
    x_branch = x_sum.astype(jnp.bfloat16)
    gate_branch = gate_sum.astype(jnp.bfloat16)
    window = jnp.concatenate([conv_state, x_branch[:, None, :]], axis=1)
    conv_out = jnp.sum(window.astype(jnp.float32) * conv_taps[None], axis=1).astype(jnp.bfloat16)
    new_conv_state = window[:, 1:, :]
    blocks = conv_out.reshape(batch_rows, recur_gate_blocks.shape[0], recur_gate_blocks.shape[1])
    recur_gate = jax.nn.sigmoid(
        jnp.einsum(
            "bhi,hij->bhj", blocks, recur_gate_blocks, preferred_element_type=jnp.float32
        ).reshape(batch_rows, channels)
    )
    input_gate = jax.nn.sigmoid(
        jnp.einsum(
            "bhi,hij->bhj", blocks, input_gate_blocks, preferred_element_type=jnp.float32
        ).reshape(batch_rows, channels)
    )
    log_decay = -decay_scale * recur_gate * decay_rate
    new_state = jnp.exp(log_decay) * recur_state + jnp.sqrt(
        -jnp.expm1(2.0 * log_decay)
    ) * input_gate * conv_out.astype(jnp.float32)
    mixer_rows = (new_state * jax.nn.gelu(gate_branch.astype(jnp.float32))).astype(jnp.bfloat16)
    mixer_part = jnp.dot(
        mixer_rows,
        lax.all_gather(out_weight, "ep", axis=1, tiled=True),
        preferred_element_type=jnp.float32,
    )
    resid = (
        tokens.astype(jnp.float32)
        + lax.psum(mixer_part.astype(jnp.bfloat16), "tp").astype(jnp.float32)
    ).astype(jnp.bfloat16)
    normed_ffn = rms_scale(resid, ffn_gain)
    router_logits = jnp.dot(normed_ffn, router_weight, preferred_element_type=jnp.float32)
    experts = router_logits.shape[1]
    expert_ids = lax.broadcasted_iota(jnp.int32, (batch_rows, TOP_K, experts), 2)
    picked = jnp.sum(
        jnp.where(routes[:, :, None] == expert_ids, router_logits[:, None, :], 0.0), axis=2
    )
    route_weight = jax.nn.sigmoid(picked - picked[:, ::-1]).astype(jnp.bfloat16)
    capacity = 2 * batch_rows * TOP_K // experts
    flat_ids = routes.reshape(batch_rows * TOP_K)
    onehot = (
        flat_ids[:, None] == lax.broadcasted_iota(jnp.int32, (batch_rows * TOP_K, experts), 1)
    ).astype(jnp.int32)
    rank = jnp.sum((jnp.cumsum(onehot, axis=0) - onehot) * onehot, axis=1)
    slot_of = (flat_ids * capacity + rank).reshape(batch_rows, TOP_K)
    slot_rows = lax.broadcasted_iota(jnp.int32, (experts * capacity, batch_rows), 0)
    slot_cols = lax.broadcasted_iota(jnp.int32, (batch_rows, experts * capacity), 1)
    dispatch = jnp.zeros((experts * capacity, batch_rows), jnp.bfloat16)
    combine = jnp.zeros((batch_rows, experts * capacity), jnp.bfloat16)
    for pick in range(TOP_K):
        dispatch = dispatch + (slot_rows == slot_of[None, :, pick]).astype(jnp.bfloat16)
        combine = combine + jnp.where(
            slot_cols == slot_of[:, pick : pick + 1],
            route_weight[:, pick : pick + 1],
            jnp.zeros((), jnp.bfloat16),
        )
    outgoing = (
        jnp.dot(dispatch, normed_ffn, preferred_element_type=jnp.float32)
        .astype(jnp.bfloat16)
        .reshape(experts, capacity, width)
    )
    gate_local = expert_gate[0]
    up_local = expert_up[0]
    down_local = expert_down[0]
    arrived_rows = lax.all_to_all(outgoing, "ep", split_axis=0, concat_axis=0, tiled=True)
    sources, items, features = arrived_rows.shape
    rows = arrived_rows.reshape(sources * items, features)
    first = jnp.dot(rows, gate_local, preferred_element_type=jnp.float32)
    second = jnp.dot(rows, up_local, preferred_element_type=jnp.float32)
    act = (jax.nn.silu(first) * second).astype(jnp.bfloat16)
    partial_value = jnp.dot(act, down_local, preferred_element_type=jnp.float32)
    total = lax.psum(partial_value.astype(jnp.bfloat16), "tp")
    returned = lax.all_to_all(
        total.reshape(sources, items, total.shape[1]), "ep", split_axis=0, concat_axis=0, tiled=True
    )
    moe = jnp.dot(
        combine,
        returned.reshape(experts * capacity, returned.shape[2]),
        preferred_element_type=jnp.float32,
    )
    dense_arrived = lax.all_to_all(normed_ffn, "ep", split_axis=1, concat_axis=0, tiled=True)
    dense_joined = jnp.concatenate([dense_gate, dense_up], axis=1)
    dense_summed = lax.psum_scatter(
        jnp.dot(dense_arrived, dense_joined, preferred_element_type=jnp.float32).astype(
            jnp.bfloat16
        ),
        "ep",
        scatter_dimension=0,
        tiled=True,
    ).astype(jnp.float32)
    dense_first = dense_summed[:, : dense_gate.shape[1]]
    dense_second = dense_summed[:, dense_gate.shape[1] :]
    dense_act = (jax.nn.silu(dense_first) * dense_second).astype(jnp.bfloat16)
    dense_part = jnp.dot(
        dense_act,
        lax.all_gather(dense_down, "ep", axis=1, tiled=True),
        preferred_element_type=jnp.float32,
    )
    branch_weight = jax.nn.sigmoid(
        jnp.dot(normed_ffn, branch_gate, preferred_element_type=jnp.float32)
    )
    dense_sum = lax.psum(dense_part.astype(jnp.bfloat16), "tp").astype(jnp.float32)
    layer_out = (resid.astype(jnp.float32) + moe + branch_weight[:, None] * dense_sum).astype(
        jnp.bfloat16
    )
    return (layer_out, new_state, new_conv_state)


def rcopy(src, dst, send, recv, ep, tp):
    return pltpu.make_async_remote_copy(
        src_ref=src,
        dst_ref=dst,
        send_sem=send,
        recv_sem=recv,
        device_id={"ep": ep, "tp": tp},
        device_id_type=pl.DeviceIdType.MESH,
    )


def dot(left, right):
    return jnp.dot(left, right, preferred_element_type=F32)


def layer_kernel(
    n, m, experts, tok_hbm, mg_hbm, fg_hbm, rt_hbm, st_hbm, cv_hbm, tap_hbm, rg_hbm, ig_hbm, dr_hbm,
    maps_hbm, iw_hbm, gw_hbm, ow_hbm, dg_hbm, du_hbm, dd_hbm, eg, eu, ed, out, st_out, cv_out,
    toks, mgain, gain, rts, state, cvs, taps, rgb, igb, decay, maps, iw, gw, ow, dg, du, dd, wg, wu, wd,
    narr, psend, precv, pkeep, rsend, rrecv, pre, bd, mask, masks, mr, mall, osend, orecv, full, nfm,
    square, lacc, accg, accu, act, dpsend, dprecv, dkeep, drsend, drrecv, dact, dall,
    ysend, yrecv, kq, xsend, xrecv, pbuf, zsend, zrecv, fblk, fin,
    lw, ts, tr, ks, kr, s2, r2, s3, r3, as_, ar, bs, br, os_, or_, zs_, zr, xs, xr, ms, mrv,
    s4, r4, s5, r5, cs, cr, es, er, ys, yr, hs_, hr, gs, gr, fs, fr,
):
    me, tp = lax.axis_index("ep"), lax.axis_index("tp")
    zs = n // 2
    z, c = me // 2, me % 2
    mate = 2 * z + 1 - c
    side = z // 2
    inner = lax.rem(z, 3) != 0
    outer = lax.rem(z, 3) == 0
    rows, width = out.shape
    q, ch = iw.shape
    g = q // m
    half = n * rows // 2
    h = dg.shape[1]

    def zp(k):
        return (z, z + 1 - 2 * lax.rem(z, 2), lax.rem(z + 2, zs), zs - 1 - z)[k]

    def tx(k):
        return (tp, tp + 1 - 2 * lax.rem(tp, 2), lax.rem(tp + 2, m), m - 1 - tp)[k]

    def lanes(e, size):
        return pl.ds(pl.multiple_of(e * size, LANES), size)

    count = [0]

    def load(src, dst):
        cp = pltpu.make_async_copy(src, dst, lw.at[count[0]])
        count[0] += 1
        cp.start()
        return cp

    sends = []

    def send(*args):
        cp = rcopy(*args)
        cp.start()
        sends.append(cp)

    def arrive(buf, sem):
        rcopy(buf, buf, sem, sem, mate, tp).wait_recv()

    ltok = load(tok_hbm, toks)
    lmain = [load(mg_hbm, mgain), load(iw_hbm, iw), load(gw_hbm, gw)]
    lrt = load(rt_hbm, rts)

    barrier = pltpu.get_barrier_semaphore()
    peers = [(lax.rem(me + d, n), tp) for d in range(1, n)]
    for k in range(1, m):
        peers += [(me, tx(k)), (mate, tx(k))]
    for ep, t in peers:
        pl.semaphore_signal(
            barrier, inc=1, device_id={"ep": ep, "tp": t}, device_id_type=pl.DeviceIdType.MESH
        )
    ltok.wait()
    pl.semaphore_wait(barrier, len(peers))

    send(toks.at[:, lanes(mate, q)], narr.at[me], ts.at[mate], tr.at[me], mate, tp)
    for k in range(1, zs):
        for core in range(2):
            to = 2 * zp(k) + core
            send(toks.at[:, lanes(to, q)], narr.at[me], ts.at[to], tr.at[me], to, tp)
    narr[me] = toks[:, lanes(me, q)]
    lrt.wait()
    lane = lax.broadcasted_iota(jnp.int32, (rows, LANES), 1)
    pair = rts[...]
    mask[...] = ((pair[:, 0:1] == lane) | (pair[:, 1:2] == lane)).astype(F32).astype(BF16)
    values = toks[...].astype(F32)
    inverse = lax.rsqrt(jnp.mean(values * values, axis=-1, keepdims=True) + epsilon)
    lsmall = [
        load(a, b)
        for a, b in (
            (cv_hbm, cvs), (tap_hbm, taps), (rg_hbm, rgb), (ig_hbm, igb), (st_hbm, state),
            (dr_hbm, decay), (fg_hbm, gain), (maps_hbm, maps),
        )
    ]
    for cp in lmain:
        cp.wait()

    def reduction(psend, precv, keep, rsend, rrecv, s2, r2, s3, r3, part):
        def first(k):
            y = part(k)
            psend[k] = y[:rows].astype(BF16)
            send(psend.at[k], precv.at[k], s2.at[k], r2.at[k], mate, tp)
            keep[k] = y[rows:]

        def second(k):
            arrive(precv.at[k], r2.at[k])
            if k == 0:
                keep[0] = keep[0] + precv[0].astype(F32)
                return
            if k < 3:
                rsend[k] = (keep[k] + precv[k].astype(F32)).astype(BF16)
            else:

                @pl.when(inner)
                def _():
                    arrive(rrecv.at[2], r3.at[2])
                    total = keep[k] + precv[k].astype(F32) + rrecv[2].astype(F32)
                    rsend[k] = total.astype(BF16)

                @pl.when(outer)
                def _():
                    rsend[k] = (keep[k] + precv[k].astype(F32)).astype(BF16)

            to = jnp.where(inner, zp(2), zp(1)) if k == 2 else zp(k)
            send(rsend.at[k], rrecv.at[k], s3.at[k], r3.at[k], 2 * to + c, tp)

        def finish():
            arrive(rrecv.at[1], r3.at[1])
            keep[0] = keep[0] + rrecv[1].astype(F32)

            @pl.when(outer)
            def _():
                arrive(rrecv.at[2], r3.at[2])
                keep[0] = keep[0] + rrecv[2].astype(F32)

            arrive(rrecv.at[3], r3.at[3])
            return keep[0] + rrecv[3].astype(F32)

        return first, second, finish

    def part(k):
        zz = zp(k)
        for core in range(2):
            slot = 2 * zz + (1 - c if core == 0 else c)
            if k or core == 0:
                arrive(narr.at[slot], tr.at[slot])
        x = jnp.concatenate([narr[2 * zz + 1 - c], narr[2 * zz + c]], axis=0)
        x = (x.astype(F32) * mgain[me]).astype(BF16)
        return jnp.concatenate([dot(x, iw[...]), dot(x, gw[...])], axis=1)

    first, second, finish = reduction(
        psend, precv, pkeep, rsend, rrecv, s2, r2, s3, r3, part
    )
    with jax.named_scope("project"):
        first(0)
        lbig = [load(a, b) for a, b in ((ow_hbm, ow), (dg_hbm, dg), (du_hbm, du), (dd_hbm, dd))]
        lexp = [load(eg, wg), load(eu, wu)]
        ldown = [load(ed.at[:, pl.ds(i * q, q)], wd.at[i]) for i in range(n)]
        for k in range(1, zs):
            first(k)
            second(k)
        second(0)
    with jax.named_scope("prepare"):
        for k in range(zs):
            for core in range(2):
                if k or core:
                    to = 2 * zp(k) + (c if core == 0 else 1 - c)
                    send(mask, masks.at[me], ks.at[to], kr.at[me], to, tp)
        masks[me] = mask[...]
        for cp in lsmall:
            cp.wait()
        per = LANES // rgb.shape[1]
        size = rgb.shape[1]
        place_r = lax.broadcasted_iota(jnp.int32, (size, LANES), 0)
        place_c = lax.broadcasted_iota(jnp.int32, (size, LANES), 1)
        for p in range(ch // LANES):
            for s in range(per):
                move = (place_c == place_r + s * size).astype(F32).astype(BF16)
                for gate, blocks in enumerate((rgb, igb)):
                    bd[p, s * size : (s + 1) * size, gate * LANES : (gate + 1) * LANES] = dot(
                        blocks[p * per + s], move
                    ).astype(BF16)
        taken = cvs.shape[1]
        total = cvs[:, 0, :].astype(F32) * taps[0:1, :]
        for j in range(1, taken):
            total += cvs[:, j, :].astype(F32) * taps[j : j + 1, :]
        pre[...] = total
        for j in range(1, taken):
            cv_out[:, j - 1, :] = cvs[:, j, :]
        accg[...] = jnp.zeros_like(accg)
        accu[...] = jnp.zeros_like(accu)
        lacc[...] = jnp.zeros_like(lacc)
        square[...] = jnp.zeros_like(square)

    with jax.named_scope("recur"):
        both = finish() * inverse
        xb = both[:, :ch].astype(BF16)
        conv = (pre[...] + xb.astype(F32) * taps[taken : taken + 1, :]).astype(BF16)
        cv_out[:, taken - 1, :] = xb
        for p in range(ch // LANES):
            at = slice(p * LANES, (p + 1) * LANES)
            gates = jax.nn.sigmoid(dot(conv[:, at], bd[p]))
            log_decay = -decay_scale * gates[:, :LANES] * decay[:, at]
            ratio = jnp.tanh(-log_decay)
            scale = jnp.sqrt(2.0 * ratio / (1.0 + ratio))
            new = jnp.exp(log_decay) * state[:, at] + scale * gates[:, LANES:] * conv[:, at].astype(F32)
            st_out[:, at] = new
            gb = both[:, ch + p * LANES : ch + (p + 1) * LANES].astype(BF16).astype(F32)
            mr[:, at] = (new * jax.nn.gelu(gb)).astype(BF16)

    with jax.named_scope("mix"):
        send(mr, mall.at[me], bs.at[0], br.at[0], mate, tp)
        for k in range(1, zs):
            send(mr, mall.at[me], as_.at[k], ar.at[k], 2 * zp(k) + c, tp)
        mall[me] = mr[...]
        for cp in lbig:
            cp.wait()

        def pass_on(k):
            slot = 2 * zp(k) + c
            arrive(mall.at[slot], ar.at[k])
            send(mall.at[slot], mall.at[slot], bs.at[k], br.at[k], mate, tp)

        def mixed(i):
            for k in (2 * i, 2 * i + 1):
                arrive(mall.at[2 * zp(k) + 1 - c], br.at[k])
            which = side if i == 0 else 1 - side
            x = mall[pl.ds(which * zs, zs)].reshape(half, ch)
            y = dot(x, ow[...]).astype(BF16)
            for t in range(m):
                osend[t, i] = y[:, t * g : (t + 1) * g]
            for k in (3, 1, 2):
                send(osend.at[tx(k), i], orecv.at[k, i], os_.at[k, i], or_.at[k, i], me, tx(k))

        def summed(i):
            which = side if i == 0 else 1 - side
            raw = narr[pl.ds(which * zs, zs), :, lanes(tp, g)].reshape(half, g)
            total = raw.astype(F32) + osend[tp, i].astype(F32)
            for k in range(1, m):
                arrive(orecv.at[k, i], or_.at[k, i])
                total += orecv[k, i].astype(F32)
            full[tp, me, which] = total.astype(BF16)

    def sided(k, i):
        return side if (k < 2) == (i == 0) else 1 - side

    def spread(k, i):
        slot, s = 2 * zp(k) + c, sided(k, i)
        at = full.at[tp, slot, s]
        for d in (1, 2):
            send(at, at, xs.at[d, k, s], xr.at[d, k, s], me, tx(d))
        send(at, at, ms.at[0, k, s], mrv.at[0, k, s], mate, tp)

    def own(i):
        at = full.at[tp, me, sided(0, i)]
        s = sided(0, i)
        for k in (3, 2, 1):
            send(at, at, zs_.at[k, s], zr.at[k, s], 2 * zp(k) + c, tp)
        spread(0, i)

    def landed(k, i):
        s = sided(k, i)
        arrive(full.at[tp, 2 * zp(k) + c, s], zr.at[k, s])
        spread(k, i)

    def relay(k, i):
        slot, s = 2 * zp(k) + c, sided(k, i)
        early = tx(1) * (1 - s) + tx(2) * s
        late = tx(2) * (1 - s) + tx(1) * s
        at = full.at[early, slot, s]
        arrive(at, xr.at[1 + s, k, s])
        send(at, at, xs.at[3, k, s], xr.at[3, k, s], me, late)
        send(at, at, ms.at[1 + s, k, s], mrv.at[1 + s, k, s], mate, tp)
        at = full.at[late, slot, s]
        arrive(at, xr.at[2 - s, k, s])
        send(at, at, ms.at[2 - s, k, s], mrv.at[2 - s, k, s], mate, tp)

    def relay_far(k, i):
        slot, s = 2 * zp(k) + c, sided(k, i)
        at = full.at[tx(3), slot, s]
        arrive(at, xr.at[3, k, s])
        send(at, at, ms.at[3, k, s], mrv.at[3, k, s], mate, tp)

    def absorb(e, s, keep):
        parts = []
        for t in range(m):
            at = slice(t * g, (t + 1) * g)
            v = full[t, e, s].astype(F32)
            square[s] += v * v
            parts.append((v * gain[e, :, at]).astype(BF16))
        x = jnp.concatenate(parts, axis=1)
        if keep:
            nfm[s] = x
        accg[s] += dot(x, wg[e])
        accu[s] += dot(x, wu[e])
        lacc[s] += lax.dot_general(
            x, maps[:, lanes(e, q)], (((1,), (1,)), ((), ())), preferred_element_type=F32
        )

    def absorb_own(k, i):
        absorb(2 * zp(k) + c, sided(k, i), k == 0)

    def absorb_mate(k, i):
        e, s = 2 * zp(k) + 1 - c, sided(k, i)
        for d in range(m):
            arrive(full.at[tx(d), e, s], mrv.at[d, k, s])
        absorb(e, s, False)

    def dpart(k):
        s = zp(k) // 2
        x = []
        for core in range(2):
            at = lax.rem(zp(k), 2) * 2 + (1 - c if core == 0 else c)
            x.append(nfm[s, pl.ds(pl.multiple_of(at * rows, rows), rows), :])
        x = jnp.concatenate(x, axis=0)
        return jnp.concatenate([dot(x, dg[...]), dot(x, du[...])], axis=1)

    dfirst, dsecond, dfinish = reduction(
        dpsend, dprecv, dkeep, drsend, drrecv, s4, r4, s5, r5, dpart
    )

    with jax.named_scope("mix_near"):
        pass_on(1)
        mixed(0)
    with jax.named_scope("mix_sum"):
        pass_on(2)
        summed(0)
        own(0)
        pass_on(3)
        mixed(1)
    with jax.named_scope("gather_near"):
        for k in range(1, zs):
            landed(k, 0)
        relay(0, 0)
        summed(1)
        own(1)
        relay_far(0, 0)
        for cp in lexp:
            cp.wait()
        absorb_own(0, 0)
        dfirst(0)
        dfirst(1)
        dsecond(1)
        for k in range(1, zs):
            relay(k, 0)
    with jax.named_scope("gather_far"):
        for k in range(1, zs):
            landed(k, 1)
            relay_far(k, 0)
        absorb_mate(0, 0)
        relay(0, 1)
        relay_far(0, 1)
        absorb_own(0, 1)
        dfirst(2)
        dsecond(2)
        dfirst(3)
        for k in range(1, zs):
            relay(k, 1)
        dsecond(3)
        dsecond(0)
        for k in range(1, zs):
            absorb_own(k, 0)
            absorb_mate(k, 0)
            relay_far(k, 1)
        absorb_mate(0, 1)
        for k in range(1, zs):
            absorb_own(k, 1)
            absorb_mate(k, 1)

    with jax.named_scope("weights"):
        inv, weight, branch = [], [], []
        for k in range(zs):
            for core in range(2):
                if k or core:
                    src = 2 * zp(k) + (c if core == 0 else 1 - c)
                    arrive(masks.at[src], kr.at[src])
        for ih in range(2):
            s = 1 - side if ih == 0 else side
            scale = lax.rsqrt(jnp.sum(square[s], axis=-1, keepdims=True) / width + epsilon)
            square[s, :, 0:1] = scale
            logits = lacc[s] * scale
            chosen = masks[pl.ds(s * zs, zs)].reshape(half, LANES)[:, : lacc.shape[2]].astype(F32)
            named = logits * chosen
            other = jnp.sum(named, axis=-1, keepdims=True) - named
            share = (jax.nn.sigmoid(logits - other) * chosen).astype(BF16).astype(F32)
            at = lax.broadcasted_iota(jnp.int32, share.shape, 1)
            weight.append(jnp.sum(jnp.where(at == me, share, 0.0), axis=-1, keepdims=True))
            branch.append(jax.nn.sigmoid(logits[:, experts : experts + 1]))
            gate = accg[s] * scale
            act[ih] = (gate * jax.nn.sigmoid(gate) * (accu[s] * scale)).astype(BF16)

    order = [lax.rem(z + 1 + i, m) for i in range(m)]

    def down(ih):
        for i in range(m):
            y = dot(act[ih], wd[2 * order[i] + 1 - c]) * weight[ih]
            ysend[i, ih] = y.astype(BF16)
            send(ysend.at[i, ih], yrecv.at[i, ih], ys.at[i, ih], yr.at[i, ih], mate, tp)
        for i in range(m):
            y = dot(act[ih], wd[2 * order[i] + c]) * weight[ih]
            for t in range(m):
                kq[i, ih, t] = y[:, t * g : (t + 1) * g]

    def forward(i, ih, extra=None):
        arrive(yrecv.at[i, ih], yr.at[i, ih])
        for t in range(m):
            at = slice(t * g, (t + 1) * g)
            total = kq[i, ih, t] + yrecv[i, ih, :, at].astype(F32)
            if extra is not None:
                total += extra[:, at]
            kq[i, ih, t] = total
            xsend[i, ih, t] = total.astype(BF16)
        for k in (3, 1, 2):
            send(
                xsend.at[i, ih, tx(k)], xrecv.at[k, i, ih], hs_.at[k, i, ih], hr.at[k, i, ih], me, tx(k)
            )

    def settle(i, ih):
        total = kq[i, ih, tp]
        for k in range(1, m):
            arrive(xrecv.at[k, i, ih], hr.at[k, i, ih])
            total += xrecv[k, i, ih].astype(F32)
        pbuf[i, ih] = total.reshape(2, 2 * rows, g)
        for k in (2, 3) if ih == 0 else (1,):
            zsend[k, i] = pbuf[i, ih, lax.rem(zp(k), 2)].astype(BF16)

    def away(k, late):
        at = pl.ds(m - 1, 1) if late else pl.ds(0, m - 1)
        j = 1 if late else 0
        send(zsend.at[k, at], zrecv.at[k, at], gs.at[k, j], gr.at[k, j], 2 * zp(k) + c, tp)

    for cp in ldown:
        cp.wait()
    with jax.named_scope("down_far"):
        down(0)
    with jax.named_scope("dense_act"):
        at = pl.ds(pl.multiple_of(lax.rem(me, zs) * rows, rows), rows)
        both = dfinish() * square[side, at, 0:1]
        lead = both[:, :h]
        dact[...] = (lead * jax.nn.sigmoid(lead) * both[:, h:]).astype(BF16)
        for k in (3, 2, 1):
            send(dact, dall.at[me], cs.at[k], cr.at[k], 2 * zp(k) + c, tp)
        send(dact, dall.at[me], es.at[0], er.at[0], mate, tp)
        dall[me] = dact[...]
    with jax.named_scope("down_near"):
        for i in range(m - 1):
            forward(i, 0)
        down(1)
        for i in range(m - 1):
            forward(i, 1)
    with jax.named_scope("dense_pass"):
        for k in range(1, zs):
            slot = 2 * zp(k) + c
            arrive(dall.at[slot], cr.at[k])
            send(dall.at[slot], dall.at[slot], es.at[k], er.at[k], mate, tp)
    with jax.named_scope("settle_far"):
        for i in range(m - 1):
            settle(i, 0)
        for k in (2, 3):
            away(k, False)
    with jax.named_scope("dense_down"):
        for k in range(zs):
            arrive(dall.at[2 * zp(k) + 1 - c], er.at[k])
        for ih in range(2):
            s = 1 - side if ih == 0 else side
            x = dall[pl.ds(s * zs, zs)].reshape(half, h)
            forward(m - 1, ih, dot(x, dd[...]) * branch[ih])
    with jax.named_scope("settle_near"):
        for i in range(m - 1):
            settle(i, 1)
        away(1, False)
        settle(m - 1, 0)
        for k in (2, 3):
            away(k, True)
        settle(m - 1, 1)
        away(1, True)
    with jax.named_scope("last_sum"):
        for k in range(1, zs):
            arrive(zrecv.at[k, pl.ds(0, m - 1)], gr.at[k, 0])
        for k in range(1, zs):
            arrive(zrecv.at[k, pl.ds(m - 1, 1)], gr.at[k, 1])
        spot = lax.rem(z, 2)
        for j in range(m):
            total = pbuf[lax.rem(j - z - 1 + 2 * m, m), 1, spot]
            for k in range(1, zs):
                total += zrecv[k, lax.rem(j - zp(k) - 1 + 2 * m, m)].astype(F32)
            resid = full[tp, 2 * j + c, side, pl.ds(pl.multiple_of(2 * rows * spot, rows), 2 * rows), :]
            total = (total + resid.astype(F32)).astype(BF16)
            for core in range(2):
                fblk[core, j] = total[core * rows : (core + 1) * rows]
    with jax.named_scope("last_gather"):
        for k in (3, 1, 2, 0):
            for dc in range(2):
                if k or dc:
                    core = c if dc == 0 else 1 - c
                    send(
                        fblk.at[core], fin.at[c, tp], fs.at[dc, k], fr.at[dc, k], 2 * z + core, tx(k)
                    )
        fin[c, tp] = fblk[c]
        for k in (0, 1, 2, 3):
            for dc in range(2):
                if k or dc:
                    core = c if dc == 0 else 1 - c
                    arrive(fin.at[core, tx(k)], fr.at[dc, k])
        for core in range(2):
            for t in range(m):
                for j in range(m):
                    base = (2 * j + core) * q + t * g
                    out[:, base : base + g] = fin[core, t, j]
    for cp in sends:
        cp.wait_send()


def in_kernel(
    n, m, tokens, recur_state, conv_state, mix_gain, in_weight, gate_weight, conv_taps,
    recur_gate_blocks, input_gate_blocks, decay_rate, out_weight, ffn_gain, router_weight, routes,
    expert_gate, expert_up, expert_down, dense_gate, dense_up, dense_down, branch_gate,
):
    rows, width = tokens.shape
    q, ch = in_weight.shape
    experts = router_weight.shape[1]
    h, f = dense_gate.shape[1], expert_down.shape[1]
    g, zs, b = q // m, n // 2, n * rows
    half = b // 2
    lines = 2 * experts
    maps = jnp.concatenate(
        [
            router_weight.T,
            branch_gate[None],
            jnp.zeros((lines - experts - 1, width), BF16),
        ],
        axis=0,
    )
    hbm = pl.BlockSpec(memory_space=pl.ANY)
    vm = pl.BlockSpec(memory_space=pltpu.VMEM)
    v = pltpu.VMEM

    def pairs(*shapes):
        return [pltpu.SemaphoreType.DMA(s) for s in shapes for _ in range(2)]

    operands = (
        tokens, mix_gain.reshape(n, 1, q), ffn_gain.reshape(n, 1, q), routes, recur_state, conv_state,
        conv_taps, recur_gate_blocks, input_gate_blocks, decay_rate.reshape(1, ch), maps,
        in_weight, gate_weight, out_weight, dense_gate, dense_up, dense_down,
        expert_gate.reshape(n, q, f), expert_up.reshape(n, q, f), expert_down[0],
    )
    return pl.pallas_call(
        functools.partial(layer_kernel, n, m, experts),
        out_shape=(
            jax.ShapeDtypeStruct((rows, width), BF16),
            jax.ShapeDtypeStruct((rows, ch), F32),
            jax.ShapeDtypeStruct(conv_state.shape, BF16),
        ),
        in_specs=[hbm] * len(operands),
        out_specs=(vm, vm, vm),
        scratch_shapes=[
            v((rows, width), BF16), v((n, 1, q), F32), v((n, 1, q), F32), v(routes.shape, jnp.int32),
            v((rows, ch), F32), v(conv_state.shape, BF16), v(conv_taps.shape, F32),
            v(recur_gate_blocks.shape, BF16), v(input_gate_blocks.shape, BF16), v((1, ch), F32),
            v((lines, width), BF16), v((q, ch), BF16), v((q, ch), BF16), v((ch, q), BF16),
            v((q, h), BF16), v((q, h), BF16), v((h, q), BF16),
            v((n, q, f), BF16), v((n, q, f), BF16), v((n, f, q), BF16),
            v((n, rows, q), BF16), v((zs, rows, 2 * ch), BF16), v((zs, rows, 2 * ch), BF16),
            v((zs, rows, 2 * ch), F32), v((zs, rows, 2 * ch), BF16), v((zs, rows, 2 * ch), BF16),
            v((rows, ch), F32), v((ch // LANES, LANES, 2 * LANES), BF16),
            v((rows, LANES), BF16), v((n, rows, LANES), BF16),
            v((rows, ch), BF16), v((n, rows, ch), BF16),
            v((m, 2, half, g), BF16), v((m, 2, half, g), BF16),
            v((m, n, 2, half, g), BF16), v((2, half, q), BF16),
            v((2, half, g), F32), v((2, half, lines), F32),
            v((2, half, f), F32), v((2, half, f), F32), v((2, half, f), BF16),
            v((zs, rows, 2 * h), BF16), v((zs, rows, 2 * h), BF16), v((zs, rows, 2 * h), F32),
            v((zs, rows, 2 * h), BF16), v((zs, rows, 2 * h), BF16),
            v((rows, h), BF16), v((n, rows, h), BF16),
            v((m, 2, half, q), BF16), v((m, 2, half, q), BF16), v((m, 2, m, half, g), F32),
            v((m, 2, m, half, g), BF16), v((m, m, 2, half, g), BF16),
            v((m, 2, 2, 2 * rows, g), F32),
            v((zs, m, 2 * rows, g), BF16), v((zs, m, 2 * rows, g), BF16),
            v((2, m, rows, g), BF16), v((2, m, m, rows, g), BF16),
            pltpu.SemaphoreType.DMA((32,)),
        ]
        + pairs(
            (n,), (n,), (zs,), (zs,), (zs,), (zs,), (m, 2), (zs, 2), (m, zs, 2), (m, zs, 2),
            (zs,), (zs,), (zs,), (zs,), (m, 2), (m, m, 2), (zs, 2), (2, m),
        ),
        compiler_params=pltpu.CompilerParams(
            collective_id=0, has_side_effects=True, vmem_limit_bytes=58 * 1024 * 1024
        ),
        name="layer",
    )(*operands)


def solution(mesh):
    in_specs = (
        P("ep", None),
        P("ep", "tp"),
        P("ep", None, "tp"),
        P(),
        P("ep", "tp"),
        P("ep", "tp"),
        P(None, "tp"),
        P("tp", None, None),
        P("tp", None, None),
        P("tp"),
        P("tp", "ep"),
        P(),
        P(),
        P("ep", None),
        P("ep", None, "tp"),
        P("ep", None, "tp"),
        P("ep", "tp", None),
        P("ep", "tp"),
        P("ep", "tp"),
        P("tp", "ep"),
        P(),
    )
    out_specs = (P("ep", None), P("ep", "tp"), P("ep", None, "tp"))
    n, m = mesh.shape["ep"], mesh.shape["tp"]

    def body(*args):
        tokens, blocks, router, dense = args[0], args[7], args[12], args[17]
        q = tokens.shape[1] // n
        fits = m == 4 and n == 2 * m and n == router.shape[1] and q % (m * LANES) == 0
        fits = fits and tokens.shape[0] % 16 == 0 and dense.shape[1] % LANES == 0
        fits = fits and LANES % blocks.shape[1] == 0
        if fits:
            return in_kernel(n, m, *args)
        return on_device(*args)

    return jax.shard_map(
        body, mesh=mesh, in_specs=in_specs, out_specs=out_specs, check_vma=False
    )
```

time: 111 us -> 99.4 us (0.90)
  Pallas kernels: 102 us -> 88 us
  local copies, waits for them, and re-layouts: 3.94 us -> 8.89 us
  other arithmetic: 3.19 us -> 1.58 us
    pallas_call x2 -> x1, Pallas kernels: 102 us -> 88 us  [in_kernel(): pl.pallas_call(functools.partial(layer_kernel, n, m, experts), out_shape=...]
    unnamed x17 -> x4, local copies, waits for them, and re-layouts: 1.71 us -> 6.4 us
    pallas_call x0 -> x1, local copies, waits for them, and re-layouts: none -> 1.71 us  [in_kernel(): pl.pallas_call(functools.partial(layer_kernel, n, m, experts), out_shape=...]
    convert_element_type x2 -> x0, other arithmetic: 1.51 us -> none  [the longest x1 0.84 us: in_kernels(): mixer_rows = (new_state * jax.nn.gelu(gate_branch.astype(F32))).astype(BF16)]
where the time goes in v1:
time: 99.4 us; the launch traced here: 99.1 us
  Pallas kernels  88 us (89%)
  local copies, waits for them, and re-layouts  8.89 us (9%)
  other arithmetic  1.58 us (2%)
    pallas_call x1, Pallas kernels, in_kernel(): pl.pallas_call(functools.partial(layer_kernel, n, m, experts), out_shape=...  88 us
    unnamed x4, local copies, waits for them, and re-layouts  6.4 us

profile of v1, /device:TPU:0, one launch (start us, length us, event | category | flops | bytes accessed | tf_op | source)
XLA Modules:
  0.0 99.1 jit_solution(14348705240014137713)
XLA Ops:
  0.6 0.1 pad.2.clone
  0.7 1.4 %copy.24.rt_hbm = s32[32,2]{1,0:T(8,128)} copy(s32[32,2]{0,1:T(2,128)} %param.34) | data formatting | bytes 512 | tf_op args[13]
  2.1 0.7 broadcast_in_dim.6
  2.8 1.6 %maximum_maximum_fusion.maps_hbm = bf16[16,4096]{1,0:T(8,128)(2,1)} fusion(bf16[1,4096]{1,0:T(2,128)(2,1)S(1)} %broadcast_in_dim.6, bf16[8,4096]{1,0:T(8,128)(2,1)} %bitcast.10, bf16[16]{0:T(256)(128)(2,1)S(1)} %pad.2.clone), kind=kLoop, calls=%fused_computation | loop fusion | flops 393216 | bytes 204832 | tf_op jit(solution)/shard_map/concatenate | solution.py:699
  4.4 1.8 %copy.25.cv_hbm = bf16[32,3,1024]{2,1,0:T(4,128)(2,1)} copy(bf16[32,3,1024]{2,0,1:T(8,128)(2,1)} %param.23) | data formatting | bytes 393216 | tf_op args[2]
  6.2 88.0 %layer.1 = (bf16[32,4096]{1,0:T(8,128)(2,1)}, f32[32,1024]{1,0:T(8,128)}, bf16[32,3,1024]{2,1,0:T(4,128)(2,1)}) custom-call(bf16[32,4096]{1,0:T(8,128)(2,1)} %tok_hbm.1, f32[8,1,512]{2,1,0:T(1,128)} %bitcast.11, f32[8,1,512]{2,1,0:T(1,128)} %bitcast.12, s32[32,2]{1,0:T(8,128)} %copy.24.rt_hbm, f32[32,1024]{1,0:T(8,128)} %st_hbm.1, ...), custom_call_target="tpu_custom_call" | custom-call | tf_op jit(solution)/shard_map/layer/pallas_call | solution.py:720
  94.1 1.7 %copy.26 = bf16[32,3,1024]{2,0,1:T(8,128)(2,1)} copy(bf16[32,3,1024]{2,1,0:T(4,128)(2,1)} %get-tuple-element.5) | data formatting | bytes 393216 | tf_op jit(solution)/shard_map/layer/pallas_call | solution.py:720
  95.9 1.7 %copy.29 = bf16[32,4096]{1,0:T(8,128)(2,1)} copy(bf16[32,4096]{1,0:T(8,128)(2,1)} %get-tuple-element.9) | data formatting | bytes 524288
  97.5 1.6 %copy.30 = f32[32,1024]{1,0:T(8,128)} copy(f32[32,1024]{1,0:T(8,128)} %get-tuple-element.10) | data formatting | bytes 262144
  (1 shorter events, 0.0 us)

commit v2 on v1

--- a/solution.py
+++ b/solution.py
@@ -183,11 +183,11 @@
 
 def layer_kernel(
     n, m, experts, tok_hbm, mg_hbm, fg_hbm, rt_hbm, st_hbm, cv_hbm, tap_hbm, rg_hbm, ig_hbm, dr_hbm,
-    maps_hbm, iw_hbm, gw_hbm, ow_hbm, dg_hbm, du_hbm, dd_hbm, eg, eu, ed, out, st_out, cv_out,
-    toks, mgain, gain, rts, state, cvs, taps, rgb, igb, decay, maps, iw, gw, ow, dg, du, dd, wg, wu, wd,
+    rw_hbm, bw_hbm, iw_hbm, gw_hbm, ow_hbm, dg_hbm, du_hbm, dd_hbm, eg, eu, ed, out, st_out, cv_out,
+    toks, mgain, gain, rts, state, cvs, taps, rgb, igb, decay, rw, bw, maps, iw, gw, ow, dg, du, dd, wg, wu, wd,
     narr, psend, precv, pkeep, rsend, rrecv, pre, bd, mask, masks, mr, mall, osend, orecv, full, nfm,
     square, lacc, accg, accu, act, dpsend, dprecv, dkeep, drsend, drrecv, dact, dall,
-    ysend, yrecv, kq, xsend, xrecv, pbuf, zsend, zrecv, fblk, fin,
+    ysend, yrecv, kq, xsend, xrecv, xjoin, pbuf, zsend, zrecv, fblk, fin,
     lw, ts, tr, ks, kr, s2, r2, s3, r3, as_, ar, bs, br, os_, or_, zs_, zr, xs, xr, ms, mrv,
     s4, r4, s5, r5, cs, cr, es, er, ys, yr, hs_, hr, gs, gr, fs, fr,
 ):
@@ -231,7 +231,8 @@
     def arrive(buf, sem):
         rcopy(buf, buf, sem, sem, mate, tp).wait_recv()
 
-    ltok = load(tok_hbm, toks)
+    with jax.named_scope('enter'):
+        ltok = load(tok_hbm, toks)
     lmain = [load(mg_hbm, mgain), load(iw_hbm, iw), load(gw_hbm, gw)]
     lrt = load(rt_hbm, rts)
 
@@ -243,30 +244,35 @@
         pl.semaphore_signal(
             barrier, inc=1, device_id={"ep": ep, "tp": t}, device_id_type=pl.DeviceIdType.MESH
         )
-    ltok.wait()
-    pl.semaphore_wait(barrier, len(peers))
+    with jax.named_scope('tokwait'):
+        ltok.wait()
+    with jax.named_scope('greet'):
+        pl.semaphore_wait(barrier, len(peers))
 
     send(toks.at[:, lanes(mate, q)], narr.at[me], ts.at[mate], tr.at[me], mate, tp)
-    for k in range(1, zs):
+    for k in (2, 1, 3):
         for core in range(2):
             to = 2 * zp(k) + core
             send(toks.at[:, lanes(to, q)], narr.at[me], ts.at[to], tr.at[me], to, tp)
     narr[me] = toks[:, lanes(me, q)]
     lrt.wait()
-    lane = lax.broadcasted_iota(jnp.int32, (rows, LANES), 1)
-    pair = rts[...]
-    mask[...] = ((pair[:, 0:1] == lane) | (pair[:, 1:2] == lane)).astype(F32).astype(BF16)
+    pair = jnp.concatenate([rts[...]] * zs, axis=1)
+    line = lax.broadcasted_iota(jnp.int32, mask.shape, 0)
+    lane = lax.broadcasted_iota(jnp.int32, mask.shape, 1) - lax.rem(me, zs) * rows
+    taken = ((pair[0:1] == line) | (pair[1:2] == line)) & (lane >= 0) & (lane < rows)
+    mask[...] = taken.astype(F32).astype(BF16)
     values = toks[...].astype(F32)
     inverse = lax.rsqrt(jnp.mean(values * values, axis=-1, keepdims=True) + epsilon)
     lsmall = [
         load(a, b)
         for a, b in (
             (cv_hbm, cvs), (tap_hbm, taps), (rg_hbm, rgb), (ig_hbm, igb), (st_hbm, state),
-            (dr_hbm, decay), (fg_hbm, gain), (maps_hbm, maps),
+            (dr_hbm, decay), (fg_hbm, gain), (rw_hbm, rw), (bw_hbm, bw),
         )
     ]
-    for cp in lmain:
-        cp.wait()
+    with jax.named_scope('lmain'):
+        for cp in lmain:
+            cp.wait()
 
     def reduction(psend, precv, keep, rsend, rrecv, s2, r2, s3, r3, part):
         def first(k):
@@ -298,7 +304,8 @@
             send(rsend.at[k], rrecv.at[k], s3.at[k], r3.at[k], 2 * to + c, tp)
 
         def finish():
-            arrive(rrecv.at[1], r3.at[1])
+            with jax.named_scope("fin1"):
+                arrive(rrecv.at[1], r3.at[1])
             keep[0] = keep[0] + rrecv[1].astype(F32)
 
             @pl.when(outer)
@@ -306,7 +313,8 @@
                 arrive(rrecv.at[2], r3.at[2])
                 keep[0] = keep[0] + rrecv[2].astype(F32)
 
-            arrive(rrecv.at[3], r3.at[3])
+            with jax.named_scope("fin3"):
+                arrive(rrecv.at[3], r3.at[3])
             return keep[0] + rrecv[3].astype(F32)
 
         return first, second, finish
@@ -329,17 +337,11 @@
         lbig = [load(a, b) for a, b in ((ow_hbm, ow), (dg_hbm, dg), (du_hbm, du), (dd_hbm, dd))]
         lexp = [load(eg, wg), load(eu, wu)]
         ldown = [load(ed.at[:, pl.ds(i * q, q)], wd.at[i]) for i in range(n)]
-        for k in range(1, zs):
+        for k in (2, 1, 3):
             first(k)
             second(k)
         second(0)
     with jax.named_scope("prepare"):
-        for k in range(zs):
-            for core in range(2):
-                if k or core:
-                    to = 2 * zp(k) + (c if core == 0 else 1 - c)
-                    send(mask, masks.at[me], ks.at[to], kr.at[me], to, tp)
-        masks[me] = mask[...]
         for cp in lsmall:
             cp.wait()
         per = LANES // rgb.shape[1]
@@ -353,13 +355,17 @@
                     bd[p, s * size : (s + 1) * size, gate * LANES : (gate + 1) * LANES] = dot(
                         blocks[p * per + s], move
                     ).astype(BF16)
-        taken = cvs.shape[1]
-        total = cvs[:, 0, :].astype(F32) * taps[0:1, :]
+        taken = cvs.shape[0]
+        total = cvs[0].astype(F32) * taps[0:1, :]
         for j in range(1, taken):
-            total += cvs[:, j, :].astype(F32) * taps[j : j + 1, :]
+            total += cvs[j].astype(F32) * taps[j : j + 1, :]
         pre[...] = total
         for j in range(1, taken):
-            cv_out[:, j - 1, :] = cvs[:, j, :]
+            cv_out[j - 1] = cvs[j]
+        for e in range(n):
+            at = slice(e * q, (e + 1) * q)
+            line = jnp.broadcast_to(bw[...].astype(F32).reshape(1, width)[:, at], (experts, q))
+            maps[:, at] = jnp.concatenate([rw[:, at].astype(F32), line], axis=0).astype(BF16)
         accg[...] = jnp.zeros_like(accg)
         accu[...] = jnp.zeros_like(accu)
         lacc[...] = jnp.zeros_like(lacc)
@@ -369,7 +375,7 @@
         both = finish() * inverse
         xb = both[:, :ch].astype(BF16)
         conv = (pre[...] + xb.astype(F32) * taps[taken : taken + 1, :]).astype(BF16)
-        cv_out[:, taken - 1, :] = xb
+        cv_out[taken - 1] = xb
         for p in range(ch // LANES):
             at = slice(p * LANES, (p + 1) * LANES)
             gates = jax.nn.sigmoid(dot(conv[:, at], bd[p]))
@@ -495,50 +501,69 @@
     with jax.named_scope("mix_near"):
         pass_on(1)
         mixed(0)
+        for k in range(zs):
+            for core in range(2):
+                if k or core:
+                    to = 2 * zp(k) + (c if core == 0 else 1 - c)
+                    send(mask, masks.at[me], ks.at[to], kr.at[me], to, tp)
+        masks[me] = mask[...]
     with jax.named_scope("mix_sum"):
         pass_on(2)
         summed(0)
+    with jax.named_scope("gather"):
         own(0)
         pass_on(3)
         mixed(1)
-    with jax.named_scope("gather_near"):
-        for k in range(1, zs):
-            landed(k, 0)
+        landed(1, 0)
         relay(0, 0)
+        landed(2, 0)
+        landed(3, 0)
+        relay(1, 0)
         summed(1)
         own(1)
+        relay(2, 0)
         relay_far(0, 0)
         for cp in lexp:
             cp.wait()
         absorb_own(0, 0)
         dfirst(0)
+        relay(3, 0)
+        relay_far(1, 0)
+        absorb_own(1, 0)
         dfirst(1)
-        dsecond(1)
-        for k in range(1, zs):
-            relay(k, 0)
-    with jax.named_scope("gather_far"):
-        for k in range(1, zs):
-            landed(k, 1)
-            relay_far(k, 0)
         absorb_mate(0, 0)
         relay(0, 1)
+        landed(1, 1)
+        relay_far(2, 0)
+        dsecond(1)
+        absorb_own(2, 0)
+        absorb_mate(1, 0)
+        landed(2, 1)
+        landed(3, 1)
+        relay(1, 1)
+        relay_far(3, 0)
+        absorb_own(3, 0)
+        absorb_mate(2, 0)
         relay_far(0, 1)
         absorb_own(0, 1)
         dfirst(2)
+        relay(2, 1)
+        absorb_mate(3, 0)
+        relay_far(1, 1)
+        absorb_own(1, 1)
+        dfirst(3)
         dsecond(2)
-        dfirst(3)
-        for k in range(1, zs):
-            relay(k, 1)
+        relay(3, 1)
+        absorb_mate(0, 1)
+        relay_far(2, 1)
+        absorb_own(2, 1)
+        absorb_mate(1, 1)
         dsecond(3)
+        relay_far(3, 1)
+        absorb_own(3, 1)
+        absorb_mate(2, 1)
         dsecond(0)
-        for k in range(1, zs):
-            absorb_own(k, 0)
-            absorb_mate(k, 0)
-            relay_far(k, 1)
-        absorb_mate(0, 1)
-        for k in range(1, zs):
-            absorb_own(k, 1)
-            absorb_mate(k, 1)
+        absorb_mate(3, 1)
 
     with jax.named_scope("weights"):
         inv, weight, branch = [], [], []
@@ -552,7 +577,7 @@
             scale = lax.rsqrt(jnp.sum(square[s], axis=-1, keepdims=True) / width + epsilon)
             square[s, :, 0:1] = scale
             logits = lacc[s] * scale
-            chosen = masks[pl.ds(s * zs, zs)].reshape(half, LANES)[:, : lacc.shape[2]].astype(F32)
+            chosen = jnp.sum(masks[pl.ds(s * zs, zs)].astype(F32), axis=0).T
             named = logits * chosen
             other = jnp.sum(named, axis=-1, keepdims=True) - named
             share = (jax.nn.sigmoid(logits - other) * chosen).astype(BF16).astype(F32)
@@ -574,6 +599,16 @@
             for t in range(m):
                 kq[i, ih, t] = y[:, t * g : (t + 1) * g]
 
+    def pass_part(k, i, ih, part, to):
+        send(part, xrecv.at[k, i, ih], hs_.at[k, i, ih], hr.at[k, i, ih], me, tx(to))
+
+    def join(i, ih):
+        lead = 1 + (i + ih) % 2
+        arrive(xrecv.at[3, i, ih], hr.at[3, i, ih])
+        total = kq[i, ih, tx(3 - lead)] + xrecv[3, i, ih].astype(F32)
+        xjoin[i, ih] = total.astype(BF16)
+        pass_part(3 - lead, i, ih, xjoin.at[i, ih], 3 - lead)
+
     def forward(i, ih, extra=None):
         arrive(yrecv.at[i, ih], yr.at[i, ih])
         for t in range(m):
@@ -583,14 +618,17 @@
                 total += extra[:, at]
             kq[i, ih, t] = total
             xsend[i, ih, t] = total.astype(BF16)
-        for k in (3, 1, 2):
-            send(
-                xsend.at[i, ih, tx(k)], xrecv.at[k, i, ih], hs_.at[k, i, ih], hr.at[k, i, ih], me, tx(k)
-            )
+        if i == m - 1:
+            for k in (3, 1, 2):
+                pass_part(k, i, ih, xsend.at[i, ih, tx(k)], k)
+        else:
+            lead = 1 + (i + ih) % 2
+            pass_part(3, i, ih, xsend.at[i, ih, tx(3)], lead)
+            pass_part(lead, i, ih, xsend.at[i, ih, tx(lead)], lead)
 
     def settle(i, ih):
         total = kq[i, ih, tp]
-        for k in range(1, m):
+        for k in range(1, m) if i == m - 1 else (1, 2):
             arrive(xrecv.at[k, i, ih], hr.at[k, i, ih])
             total += xrecv[k, i, ih].astype(F32)
         pbuf[i, ih] = total.reshape(2, 2 * rows, g)
@@ -621,12 +659,15 @@
         down(1)
         for i in range(m - 1):
             forward(i, 1)
+            join(i, 0)
     with jax.named_scope("dense_pass"):
         for k in range(1, zs):
             slot = 2 * zp(k) + c
             arrive(dall.at[slot], cr.at[k])
             send(dall.at[slot], dall.at[slot], es.at[k], er.at[k], mate, tp)
     with jax.named_scope("settle_far"):
+        for i in range(m - 1):
+            join(i, 1)
         for i in range(m - 1):
             settle(i, 0)
         for k in (2, 3):
@@ -696,14 +737,7 @@
     g, zs, b = q // m, n // 2, n * rows
     half = b // 2
     lines = 2 * experts
-    maps = jnp.concatenate(
-        [
-            router_weight.T,
-            branch_gate[None],
-            jnp.zeros((lines - experts - 1, width), BF16),
-        ],
-        axis=0,
-    )
+    past = (conv_state.shape[1], rows, ch)
     hbm = pl.BlockSpec(memory_space=pl.ANY)
     vm = pl.BlockSpec(memory_space=pltpu.VMEM)
     v = pltpu.VMEM
@@ -712,31 +746,33 @@
         return [pltpu.SemaphoreType.DMA(s) for s in shapes for _ in range(2)]
 
     operands = (
-        tokens, mix_gain.reshape(n, 1, q), ffn_gain.reshape(n, 1, q), routes, recur_state, conv_state,
-        conv_taps, recur_gate_blocks, input_gate_blocks, decay_rate.reshape(1, ch), maps,
+        tokens, mix_gain.reshape(n, 1, q), ffn_gain.reshape(n, 1, q), routes.T, recur_state,
+        conv_state.transpose(1, 0, 2), conv_taps, recur_gate_blocks, input_gate_blocks,
+        decay_rate.reshape(1, ch), router_weight.T, branch_gate,
         in_weight, gate_weight, out_weight, dense_gate, dense_up, dense_down,
         expert_gate.reshape(n, q, f), expert_up.reshape(n, q, f), expert_down[0],
     )
-    return pl.pallas_call(
+    results = (
+        jax.ShapeDtypeStruct((rows, width), BF16),
+        jax.ShapeDtypeStruct((rows, ch), F32),
+        jax.ShapeDtypeStruct(past, BF16),
+    )
+    layer_out, new_state, window = pl.pallas_call(
         functools.partial(layer_kernel, n, m, experts),
-        out_shape=(
-            jax.ShapeDtypeStruct((rows, width), BF16),
-            jax.ShapeDtypeStruct((rows, ch), F32),
-            jax.ShapeDtypeStruct(conv_state.shape, BF16),
-        ),
+        out_shape=tuple(pltpu.VMEM(r.shape, r.dtype) for r in results),
         in_specs=[hbm] * len(operands),
         out_specs=(vm, vm, vm),
         scratch_shapes=[
-            v((rows, width), BF16), v((n, 1, q), F32), v((n, 1, q), F32), v(routes.shape, jnp.int32),
-            v((rows, ch), F32), v(conv_state.shape, BF16), v(conv_taps.shape, F32),
+            v((rows, width), BF16), v((n, 1, q), F32), v((n, 1, q), F32), v(routes.shape[::-1], jnp.int32),
+            v((rows, ch), F32), v(past, BF16), v(conv_taps.shape, F32),
             v(recur_gate_blocks.shape, BF16), v(input_gate_blocks.shape, BF16), v((1, ch), F32),
-            v((lines, width), BF16), v((q, ch), BF16), v((q, ch), BF16), v((ch, q), BF16),
+            v((experts, width), BF16), v((width,), BF16), v((lines, width), BF16), v((q, ch), BF16), v((q, ch), BF16), v((ch, q), BF16),
             v((q, h), BF16), v((q, h), BF16), v((h, q), BF16),
             v((n, q, f), BF16), v((n, q, f), BF16), v((n, f, q), BF16),
             v((n, rows, q), BF16), v((zs, rows, 2 * ch), BF16), v((zs, rows, 2 * ch), BF16),
             v((zs, rows, 2 * ch), F32), v((zs, rows, 2 * ch), BF16), v((zs, rows, 2 * ch), BF16),
             v((rows, ch), F32), v((ch // LANES, LANES, 2 * LANES), BF16),
-            v((rows, LANES), BF16), v((n, rows, LANES), BF16),
+            v((lines, half), BF16), v((n, lines, half), BF16),
             v((rows, ch), BF16), v((n, rows, ch), BF16),
             v((m, 2, half, g), BF16), v((m, 2, half, g), BF16),
             v((m, n, 2, half, g), BF16), v((2, half, q), BF16),
@@ -746,7 +782,7 @@
             v((zs, rows, 2 * h), BF16), v((zs, rows, 2 * h), BF16),
             v((rows, h), BF16), v((n, rows, h), BF16),
             v((m, 2, half, q), BF16), v((m, 2, half, q), BF16), v((m, 2, m, half, g), F32),
-            v((m, 2, m, half, g), BF16), v((m, m, 2, half, g), BF16),
+            v((m, 2, m, half, g), BF16), v((m, m, 2, half, g), BF16), v((m - 1, 2, half, g), BF16),
             v((m, 2, 2, 2 * rows, g), F32),
             v((zs, m, 2 * rows, g), BF16), v((zs, m, 2 * rows, g), BF16),
             v((2, m, rows, g), BF16), v((2, m, m, rows, g), BF16),
@@ -761,6 +797,7 @@
         ),
         name="layer",
     )(*operands)
+    return (layer_out, new_state, window.transpose(1, 0, 2))
 
 
 def solution(mesh):

time: 99.4 us -> 83.7 us (0.84)
  Pallas kernels: 88 us -> 80.9 us
  local copies, waits for them, and re-layouts: 8.89 us -> 2.04 us
  other arithmetic: 1.58 us -> 0 us
    pallas_call x1, Pallas kernels: 88 us -> 80.9 us  [in_kernel(): pl.pallas_call(functools.partial(layer_kernel, n, m, experts), out_shape=...]
    unnamed x4 -> x3, local copies, waits for them, and re-layouts: 6.4 us -> 2.04 us
    pallas_call x1 -> x0, local copies, waits for them, and re-layouts: 1.71 us -> none  [in_kernel(): pl.pallas_call(functools.partial(layer_kernel, n, m, experts), out_shape=...]
    concatenate x1 -> x0, other arithmetic: 1.58 us -> none  [in_kernel(): jnp.concatenate([router_weight.T, branch_gate[None], jnp.zeros((lines - e...]
where the time goes in v2:
time: 83.7 us; the launch traced here: 83.6 us
  Pallas kernels  80.9 us (97%)
  local copies, waits for them, and re-layouts  2.04 us (2%)
    pallas_call x1, Pallas kernels, in_kernel(): pl.pallas_call(functools.partial(layer_kernel, n, m, experts), out_shape=...  80.9 us
    unnamed x3, local copies, waits for them, and re-layouts  2.04 us

profile of v2, /device:TPU:0, one launch (start us, length us, event | category | flops | bytes accessed | tf_op | source)
XLA Modules:
  0.0 83.6 jit_solution(13469723425279587645)
XLA Ops:
  0.6 80.9 %layer.1 = (bf16[32,4096]{1,0:T(8,128)(2,1)S(1)}, f32[32,1024]{1,0:T(8,128)S(1)}, bf16[3,32,1024]{2,1,0:T(8,128)(2,1)S(1)}) custom-call(bf16[32,4096]{1,0:T(8,128)(2,1)} %tok_hbm.1, f32[8,1,512]{2,1,0:T(1,128)} %bitcast.16, f32[8,1,512]{2,1,0:T(1,128)} %bitcast.17, s32[2,32]{1,0:T(2,128)} %bitcast.19, f32[32,1024]{1,0:T(8,128)} %st_hbm.1, ...), custom_call_target="tpu_custom_call" | custom-call | tf_op jit(solution)/shard_map/layer/pallas_call | solution.py:760
  81.6 0.7 copy.27
  82.3 0.7 copy.28
  82.9 0.7 copy.29

commit v3 on v2

--- a/solution.py
+++ b/solution.py
@@ -188,8 +188,7 @@
     narr, psend, precv, pkeep, rsend, rrecv, pre, bd, mask, masks, mr, mall, osend, orecv, full, nfm,
     square, lacc, accg, accu, act, dpsend, dprecv, dkeep, drsend, drrecv, dact, dall,
     ysend, yrecv, kq, xsend, xrecv, xjoin, pbuf, zsend, zrecv, fblk, fin,
-    lw, ts, tr, ks, kr, s2, r2, s3, r3, as_, ar, bs, br, os_, or_, zs_, zr, xs, xr, ms, mrv,
-    s4, r4, s5, r5, cs, cr, es, er, ys, yr, hs_, hr, gs, gr, fs, fr,
+    lw, sent, tr, kr, r2, r3, ar, br, or_, zr, xr, mrv, r4, r5, cr, er, yr, hr, gr, fr,
 ):
     me, tp = lax.axis_index("ep"), lax.axis_index("tp")
     zs = n // 2
@@ -223,8 +222,8 @@
 
     sends = []
 
-    def send(*args):
-        cp = rcopy(*args)
+    def send(src, dst, recv, ep, t):
+        cp = rcopy(src, dst, sent.at[0], recv, ep, t)
         cp.start()
         sends.append(cp)
 
@@ -249,11 +248,11 @@
     with jax.named_scope('greet'):
         pl.semaphore_wait(barrier, len(peers))
 
-    send(toks.at[:, lanes(mate, q)], narr.at[me], ts.at[mate], tr.at[me], mate, tp)
+    send(toks.at[:, lanes(mate, q)], narr.at[me], tr.at[me], mate, tp)
     for k in (2, 1, 3):
         for core in range(2):
             to = 2 * zp(k) + core
-            send(toks.at[:, lanes(to, q)], narr.at[me], ts.at[to], tr.at[me], to, tp)
+            send(toks.at[:, lanes(to, q)], narr.at[me], tr.at[me], to, tp)
     narr[me] = toks[:, lanes(me, q)]
     lrt.wait()
     pair = jnp.concatenate([rts[...]] * zs, axis=1)
@@ -274,34 +273,46 @@
         for cp in lmain:
             cp.wait()
 
-    def reduction(psend, precv, keep, rsend, rrecv, s2, r2, s3, r3, part):
+    def reduction(psend, precv, keep, rsend, rrecv, r2, r3, part):
         def first(k):
             y = part(k)
             psend[k] = y[:rows].astype(BF16)
-            send(psend.at[k], precv.at[k], s2.at[k], r2.at[k], mate, tp)
+            send(psend.at[k], precv.at[k], r2.at[k], mate, tp)
             keep[k] = y[rows:]
+
+        def target(k):
+            return jnp.where(inner, zp(2), zp(1)) if k == 2 else zp(k)
+
+        def out_of(k):
+            return rcopy(
+                rsend.at[k], rrecv.at[k], sent.at[0], r3.at[k], 2 * target(k) + c, tp
+            )
 
         def second(k):
             arrive(precv.at[k], r2.at[k])
             if k == 0:
                 keep[0] = keep[0] + precv[0].astype(F32)
                 return
-            if k < 3:
-                rsend[k] = (keep[k] + precv[k].astype(F32)).astype(BF16)
-            else:
-
-                @pl.when(inner)
-                def _():
-                    arrive(rrecv.at[2], r3.at[2])
-                    total = keep[k] + precv[k].astype(F32) + rrecv[2].astype(F32)
-                    rsend[k] = total.astype(BF16)
-
-                @pl.when(outer)
-                def _():
-                    rsend[k] = (keep[k] + precv[k].astype(F32)).astype(BF16)
-
-            to = jnp.where(inner, zp(2), zp(1)) if k == 2 else zp(k)
-            send(rsend.at[k], rrecv.at[k], s3.at[k], r3.at[k], 2 * to + c, tp)
+            rsend[k] = (keep[k] + precv[k].astype(F32)).astype(BF16)
+            send(rsend.at[k], rrecv.at[k], r3.at[k], 2 * target(k) + c, tp)
+
+        def last_outer():
+            @pl.when(outer)
+            def _():
+                arrive(precv.at[3], r2.at[3])
+                rsend[3] = (keep[3] + precv[3].astype(F32)).astype(BF16)
+                out_of(3).start()
+
+        def last_inner():
+            @pl.when(inner)
+            def _():
+                arrive(precv.at[3], r2.at[3])
+                arrive(rrecv.at[2], r3.at[2])
+                total = keep[3] + precv[3].astype(F32) + rrecv[2].astype(F32)
+                rsend[3] = total.astype(BF16)
+                out_of(3).start()
+
+            sends.append(out_of(3))
 
         def finish():
             with jax.named_scope("fin1"):
@@ -317,7 +328,7 @@
                 arrive(rrecv.at[3], r3.at[3])
             return keep[0] + rrecv[3].astype(F32)
 
-        return first, second, finish
+        return first, second, last_outer, last_inner, finish
 
     def part(k):
         zz = zp(k)
@@ -329,17 +340,20 @@
         x = (x.astype(F32) * mgain[me]).astype(BF16)
         return jnp.concatenate([dot(x, iw[...]), dot(x, gw[...])], axis=1)
 
-    first, second, finish = reduction(
-        psend, precv, pkeep, rsend, rrecv, s2, r2, s3, r3, part
+    first, second, last_outer, last_inner, finish = reduction(
+        psend, precv, pkeep, rsend, rrecv, r2, r3, part
     )
     with jax.named_scope("project"):
         first(0)
         lbig = [load(a, b) for a, b in ((ow_hbm, ow), (dg_hbm, dg), (du_hbm, du), (dd_hbm, dd))]
         lexp = [load(eg, wg), load(eu, wu)]
         ldown = [load(ed.at[:, pl.ds(i * q, q)], wd.at[i]) for i in range(n)]
-        for k in (2, 1, 3):
+        for k in (2, 1):
             first(k)
             second(k)
+        first(3)
+        last_outer()
+        last_inner()
         second(0)
     with jax.named_scope("prepare"):
         for cp in lsmall:
@@ -388,9 +402,9 @@
             mr[:, at] = (new * jax.nn.gelu(gb)).astype(BF16)
 
     with jax.named_scope("mix"):
-        send(mr, mall.at[me], bs.at[0], br.at[0], mate, tp)
+        send(mr, mall.at[me], br.at[0], mate, tp)
         for k in range(1, zs):
-            send(mr, mall.at[me], as_.at[k], ar.at[k], 2 * zp(k) + c, tp)
+            send(mr, mall.at[me], ar.at[k], 2 * zp(k) + c, tp)
         mall[me] = mr[...]
         for cp in lbig:
             cp.wait()
@@ -398,7 +412,7 @@
         def pass_on(k):
             slot = 2 * zp(k) + c
             arrive(mall.at[slot], ar.at[k])
-            send(mall.at[slot], mall.at[slot], bs.at[k], br.at[k], mate, tp)
+            send(mall.at[slot], mall.at[slot], br.at[k], mate, tp)
 
         def mixed(i):
             for k in (2 * i, 2 * i + 1):
@@ -409,7 +423,7 @@
             for t in range(m):
                 osend[t, i] = y[:, t * g : (t + 1) * g]
             for k in (3, 1, 2):
-                send(osend.at[tx(k), i], orecv.at[k, i], os_.at[k, i], or_.at[k, i], me, tx(k))
+                send(osend.at[tx(k), i], orecv.at[k, i], or_.at[k, i], me, tx(k))
 
         def summed(i):
             which = side if i == 0 else 1 - side
@@ -420,21 +434,23 @@
                 total += orecv[k, i].astype(F32)
             full[tp, me, which] = total.astype(BF16)
 
+    direct = [(k, 1) for k in range(zs)]
+
     def sided(k, i):
         return side if (k < 2) == (i == 0) else 1 - side
 
     def spread(k, i):
         slot, s = 2 * zp(k) + c, sided(k, i)
         at = full.at[tp, slot, s]
-        for d in (1, 2):
-            send(at, at, xs.at[d, k, s], xr.at[d, k, s], me, tx(d))
-        send(at, at, ms.at[0, k, s], mrv.at[0, k, s], mate, tp)
+        for d in (3, 1, 2) if (k, i) in direct else (1, 2):
+            send(at, at, xr.at[d, k, s], me, tx(d))
+        send(at, at, mrv.at[0, k, s], mate, tp)
 
     def own(i):
         at = full.at[tp, me, sided(0, i)]
         s = sided(0, i)
         for k in (3, 2, 1):
-            send(at, at, zs_.at[k, s], zr.at[k, s], 2 * zp(k) + c, tp)
+            send(at, at, zr.at[k, s], 2 * zp(k) + c, tp)
         spread(0, i)
 
     def landed(k, i):
@@ -448,17 +464,18 @@
         late = tx(2) * (1 - s) + tx(1) * s
         at = full.at[early, slot, s]
         arrive(at, xr.at[1 + s, k, s])
-        send(at, at, xs.at[3, k, s], xr.at[3, k, s], me, late)
-        send(at, at, ms.at[1 + s, k, s], mrv.at[1 + s, k, s], mate, tp)
+        if (k, i) not in direct:
+            send(at, at, xr.at[3, k, s], me, late)
+        send(at, at, mrv.at[1 + s, k, s], mate, tp)
         at = full.at[late, slot, s]
         arrive(at, xr.at[2 - s, k, s])
-        send(at, at, ms.at[2 - s, k, s], mrv.at[2 - s, k, s], mate, tp)
+        send(at, at, mrv.at[2 - s, k, s], mate, tp)
 
     def relay_far(k, i):
         slot, s = 2 * zp(k) + c, sided(k, i)
         at = full.at[tx(3), slot, s]
         arrive(at, xr.at[3, k, s])
-        send(at, at, ms.at[3, k, s], mrv.at[3, k, s], mate, tp)
+        send(at, at, mrv.at[3, k, s], mate, tp)
 
     def absorb(e, s, keep):
         parts = []
@@ -494,8 +511,8 @@
         x = jnp.concatenate(x, axis=0)
         return jnp.concatenate([dot(x, dg[...]), dot(x, du[...])], axis=1)
 
-    dfirst, dsecond, dfinish = reduction(
-        dpsend, dprecv, dkeep, drsend, drrecv, s4, r4, s5, r5, dpart
+    dfirst, dsecond, dlast_outer, dlast_inner, dfinish = reduction(
+        dpsend, dprecv, dkeep, drsend, drrecv, r4, r5, dpart
     )
 
     with jax.named_scope("mix_near"):
@@ -505,7 +522,7 @@
             for core in range(2):
                 if k or core:
                     to = 2 * zp(k) + (c if core == 0 else 1 - c)
-                    send(mask, masks.at[me], ks.at[to], kr.at[me], to, tp)
+                    send(mask, masks.at[me], kr.at[me], to, tp)
         masks[me] = mask[...]
     with jax.named_scope("mix_sum"):
         pass_on(2)
@@ -529,13 +546,19 @@
         dfirst(0)
         relay(3, 0)
         relay_far(1, 0)
+        dfirst(1)
         absorb_own(1, 0)
-        dfirst(1)
         absorb_mate(0, 0)
         relay(0, 1)
+        relay_far(0, 1)
+        absorb_own(0, 1)
+        dfirst(2)
+        dsecond(1)
+        dfirst(3)
         landed(1, 1)
         relay_far(2, 0)
-        dsecond(1)
+        dsecond(2)
+        dlast_outer()
         absorb_own(2, 0)
         absorb_mate(1, 0)
         landed(2, 1)
@@ -544,48 +567,56 @@
         relay_far(3, 0)
         absorb_own(3, 0)
         absorb_mate(2, 0)
-        relay_far(0, 1)
-        absorb_own(0, 1)
-        dfirst(2)
         relay(2, 1)
         absorb_mate(3, 0)
         relay_far(1, 1)
         absorb_own(1, 1)
-        dfirst(3)
-        dsecond(2)
         relay(3, 1)
+        dlast_inner()
         absorb_mate(0, 1)
         relay_far(2, 1)
         absorb_own(2, 1)
         absorb_mate(1, 1)
-        dsecond(3)
         relay_far(3, 1)
         absorb_own(3, 1)
         absorb_mate(2, 1)
         dsecond(0)
         absorb_mate(3, 1)
 
-    with jax.named_scope("weights"):
-        inv, weight, branch = [], [], []
+    scale = []
+    with jax.named_scope("dense_act"):
+        for s in (1 - side, side):
+            scale.append(
+                lax.rsqrt(jnp.sum(square[s], axis=-1, keepdims=True) / width + epsilon)
+            )
+            square[s, :, 0:1] = scale[-1]
+        at = pl.ds(pl.multiple_of(lax.rem(me, zs) * rows, rows), rows)
+        both = dfinish() * square[side, at, 0:1]
+        first_half = both[:, :h]
+        dact[...] = (first_half * jax.nn.sigmoid(first_half) * both[:, h:]).astype(BF16)
+        for k in (3, 2, 1):
+            send(dact, dall.at[me], cr.at[k], 2 * zp(k) + c, tp)
+        send(dact, dall.at[me], er.at[0], mate, tp)
+        dall[me] = dact[...]
         for k in range(zs):
             for core in range(2):
                 if k or core:
                     src = 2 * zp(k) + (c if core == 0 else 1 - c)
                     arrive(masks.at[src], kr.at[src])
-        for ih in range(2):
-            s = 1 - side if ih == 0 else side
-            scale = lax.rsqrt(jnp.sum(square[s], axis=-1, keepdims=True) / width + epsilon)
-            square[s, :, 0:1] = scale
-            logits = lacc[s] * scale
-            chosen = jnp.sum(masks[pl.ds(s * zs, zs)].astype(F32), axis=0).T
-            named = logits * chosen
-            other = jnp.sum(named, axis=-1, keepdims=True) - named
-            share = (jax.nn.sigmoid(logits - other) * chosen).astype(BF16).astype(F32)
-            at = lax.broadcasted_iota(jnp.int32, share.shape, 1)
-            weight.append(jnp.sum(jnp.where(at == me, share, 0.0), axis=-1, keepdims=True))
-            branch.append(jax.nn.sigmoid(logits[:, experts : experts + 1]))
-            gate = accg[s] * scale
-            act[ih] = (gate * jax.nn.sigmoid(gate) * (accu[s] * scale)).astype(BF16)
+    weight, branch = [], []
+
+    def activate(ih):
+        s = 1 - side if ih == 0 else side
+        logits = lacc[s] * scale[ih]
+        chosen = jnp.sum(masks[pl.ds(s * zs, zs)].astype(F32), axis=0).T
+        named = logits * chosen
+        other = jnp.sum(named, axis=-1, keepdims=True) - named
+        share = (jax.nn.sigmoid(logits - other) * chosen).astype(BF16).astype(F32)
+        at = lax.broadcasted_iota(jnp.int32, share.shape, 1)
+        weight.append(jnp.sum(jnp.where(at == me, share, 0.0), axis=-1, keepdims=True))
+        branch.append(jax.nn.sigmoid(logits[:, experts : experts + 1]))
+        gate = accg[s] * scale[ih]
+        act[ih] = (gate * jax.nn.sigmoid(gate) * (accu[s] * scale[ih])).astype(BF16)
 
     order = [lax.rem(z + 1 + i, m) for i in range(m)]
 
@@ -593,14 +624,16 @@
         for i in range(m):
             y = dot(act[ih], wd[2 * order[i] + 1 - c]) * weight[ih]
             ysend[i, ih] = y.astype(BF16)
-            send(ysend.at[i, ih], yrecv.at[i, ih], ys.at[i, ih], yr.at[i, ih], mate, tp)
+            send(ysend.at[i, ih], yrecv.at[i, ih], yr.at[i, ih], mate, tp)
         for i in range(m):
             y = dot(act[ih], wd[2 * order[i] + c]) * weight[ih]
             for t in range(m):
                 kq[i, ih, t] = y[:, t * g : (t + 1) * g]
 
+    joined = [(i, 1) for i in range(m - 1)]
+
     def pass_part(k, i, ih, part, to):
-        send(part, xrecv.at[k, i, ih], hs_.at[k, i, ih], hr.at[k, i, ih], me, tx(to))
+        send(part, xrecv.at[k, i, ih], hr.at[k, i, ih], me, tx(to))
 
     def join(i, ih):
         lead = 1 + (i + ih) % 2
@@ -618,7 +651,7 @@
                 total += extra[:, at]
             kq[i, ih, t] = total
             xsend[i, ih, t] = total.astype(BF16)
-        if i == m - 1:
+        if (i, ih) not in joined:
             for k in (3, 1, 2):
                 pass_part(k, i, ih, xsend.at[i, ih, tx(k)], k)
         else:
@@ -628,71 +661,92 @@
 
     def settle(i, ih):
         total = kq[i, ih, tp]
-        for k in range(1, m) if i == m - 1 else (1, 2):
+        for k in (1, 2) if (i, ih) in joined else range(1, m):
             arrive(xrecv.at[k, i, ih], hr.at[k, i, ih])
             total += xrecv[k, i, ih].astype(F32)
         pbuf[i, ih] = total.reshape(2, 2 * rows, g)
         for k in (2, 3) if ih == 0 else (1,):
             zsend[k, i] = pbuf[i, ih, lax.rem(zp(k), 2)].astype(BF16)
 
-    def away(k, late):
-        at = pl.ds(m - 1, 1) if late else pl.ds(0, m - 1)
-        j = 1 if late else 0
-        send(zsend.at[k, at], zrecv.at[k, at], gs.at[k, j], gr.at[k, j], 2 * zp(k) + c, tp)
+    def away(k, i):
+        send(zsend.at[k, i], zrecv.at[k, i], gr.at[k, i], 2 * zp(k) + c, tp)
 
     for cp in ldown:
         cp.wait()
     with jax.named_scope("down_far"):
+        activate(0)
         down(0)
-    with jax.named_scope("dense_act"):
-        at = pl.ds(pl.multiple_of(lax.rem(me, zs) * rows, rows), rows)
-        both = dfinish() * square[side, at, 0:1]
-        lead = both[:, :h]
-        dact[...] = (lead * jax.nn.sigmoid(lead) * both[:, h:]).astype(BF16)
-        for k in (3, 2, 1):
-            send(dact, dall.at[me], cs.at[k], cr.at[k], 2 * zp(k) + c, tp)
-        send(dact, dall.at[me], es.at[0], er.at[0], mate, tp)
-        dall[me] = dact[...]
-    with jax.named_scope("down_near"):
-        for i in range(m - 1):
-            forward(i, 0)
-        down(1)
-        for i in range(m - 1):
-            forward(i, 1)
-            join(i, 0)
-    with jax.named_scope("dense_pass"):
-        for k in range(1, zs):
+        activate(1)
+    def dense_pass():
+        for k in (1, 2, 3):
             slot = 2 * zp(k) + c
             arrive(dall.at[slot], cr.at[k])
-            send(dall.at[slot], dall.at[slot], es.at[k], er.at[k], mate, tp)
-    with jax.named_scope("settle_far"):
-        for i in range(m - 1):
-            join(i, 1)
-        for i in range(m - 1):
-            settle(i, 0)
-        for k in (2, 3):
-            away(k, False)
-    with jax.named_scope("dense_down"):
+            send(dall.at[slot], dall.at[slot], er.at[k], mate, tp)
+
+    def dense_ready():
         for k in range(zs):
             arrive(dall.at[2 * zp(k) + 1 - c], er.at[k])
-        for ih in range(2):
-            s = 1 - side if ih == 0 else side
-            x = dall[pl.ds(s * zs, zs)].reshape(half, h)
-            forward(m - 1, ih, dot(x, dd[...]) * branch[ih])
-    with jax.named_scope("settle_near"):
-        for i in range(m - 1):
-            settle(i, 1)
-        away(1, False)
-        settle(m - 1, 0)
-        for k in (2, 3):
-            away(k, True)
-        settle(m - 1, 1)
-        away(1, True)
+
+    def dense_forward(ih):
+        s = 1 - side if ih == 0 else side
+        x = dall[pl.ds(s * zs, zs)].reshape(half, h)
+        forward(m - 1, ih, dot(x, dd[...]) * branch[ih])
+
+    def leave(i, ih):
+        settle(i, ih)
+        for k in (3, 2) if ih == 0 else (1,):
+            away(k, i)
+
+    with jax.named_scope("tail"):
+        with jax.named_scope("f00"):
+            forward(0, 0)
+        with jax.named_scope("f10"):
+            forward(1, 0)
+        with jax.named_scope("f20"):
+            forward(2, 0)
+        with jax.named_scope("d1"):
+            down(1)
+        with jax.named_scope("f01"):
+            forward(0, 1)
+        with jax.named_scope("f11"):
+            forward(1, 1)
+        with jax.named_scope("f21"):
+            forward(2, 1)
+        with jax.named_scope("l00"):
+            leave(0, 0)
+        with jax.named_scope("dp"):
+            dense_pass()
+        with jax.named_scope("l10"):
+            leave(1, 0)
+        with jax.named_scope("l20"):
+            leave(2, 0)
+        with jax.named_scope("dr"):
+            dense_ready()
+        with jax.named_scope("df0"):
+            dense_forward(0)
+        with jax.named_scope("df1"):
+            dense_forward(1)
+        with jax.named_scope("j01"):
+            join(0, 1)
+        with jax.named_scope("j11"):
+            join(1, 1)
+        with jax.named_scope("j21"):
+            join(2, 1)
+        with jax.named_scope("l30"):
+            leave(3, 0)
+        with jax.named_scope("l01"):
+            leave(0, 1)
+        with jax.named_scope("l11"):
+            leave(1, 1)
+        with jax.named_scope("l21"):
+            leave(2, 1)
+        with jax.named_scope("l31"):
+            leave(3, 1)
+
     with jax.named_scope("last_sum"):
         for k in range(1, zs):
-            arrive(zrecv.at[k, pl.ds(0, m - 1)], gr.at[k, 0])
-        for k in range(1, zs):
-            arrive(zrecv.at[k, pl.ds(m - 1, 1)], gr.at[k, 1])
+            for i in range(m):
+                arrive(zrecv.at[k, i], gr.at[k, i])
         spot = lax.rem(z, 2)
         for j in range(m):
             total = pbuf[lax.rem(j - z - 1 + 2 * m, m), 1, spot]
@@ -708,7 +762,7 @@
                 if k or dc:
                     core = c if dc == 0 else 1 - c
                     send(
-                        fblk.at[core], fin.at[c, tp], fs.at[dc, k], fr.at[dc, k], 2 * z + core, tx(k)
+                        fblk.at[core], fin.at[c, tp], fr.at[dc, k], 2 * z + core, tx(k)
                     )
         fin[c, tp] = fblk[c]
         for k in (0, 1, 2, 3):
@@ -721,8 +775,20 @@
                 for j in range(m):
                     base = (2 * j + core) * q + t * g
                     out[:, base : base + g] = fin[core, t, j]
-    for cp in sends:
-        cp.wait_send()
+    with jax.named_scope("drain"):
+        for cp in sends:
+            cp.wait_send()
+
+
+def deliver_kernel(a, b, c, to_a, to_b, to_c, sems):
+    copies = [
+        pltpu.make_async_copy(src, dst, sems.at[i])
+        for i, (src, dst) in enumerate(((a, to_a), (b, to_b), (c, to_c)))
+    ]
+    for cp in copies:
+        cp.start()
+    for cp in copies:
+        cp.wait()
 
 
 def in_kernel(
@@ -742,8 +808,8 @@
     vm = pl.BlockSpec(memory_space=pltpu.VMEM)
     v = pltpu.VMEM
 
-    def pairs(*shapes):
-        return [pltpu.SemaphoreType.DMA(s) for s in shapes for _ in range(2)]
+    def flags(*shapes):
+        return [pltpu.SemaphoreType.DMA(s) for s in shapes]
 
     operands = (
         tokens, mix_gain.reshape(n, 1, q), ffn_gain.reshape(n, 1, q), routes.T, recur_state,
@@ -786,17 +852,25 @@
             v((m, 2, 2, 2 * rows, g), F32),
             v((zs, m, 2 * rows, g), BF16), v((zs, m, 2 * rows, g), BF16),
             v((2, m, rows, g), BF16), v((2, m, m, rows, g), BF16),
-            pltpu.SemaphoreType.DMA((32,)),
         ]
-        + pairs(
-            (n,), (n,), (zs,), (zs,), (zs,), (zs,), (m, 2), (zs, 2), (m, zs, 2), (m, zs, 2),
-            (zs,), (zs,), (zs,), (zs,), (m, 2), (m, m, 2), (zs, 2), (2, m),
+        + flags(
+            (32,), (1,), (n,), (n,), (zs,), (zs,), (zs,), (zs,), (m, 2), (zs, 2), (m, zs, 2), (m, zs, 2),
+            (zs,), (zs,), (zs,), (zs,), (m, 2), (m, m, 2), (zs, m), (2, m),
         ),
         compiler_params=pltpu.CompilerParams(
             collective_id=0, has_side_effects=True, vmem_limit_bytes=58 * 1024 * 1024
         ),
         name="layer",
     )(*operands)
+    held = [pltpu.with_memory_space_constraint(a, pltpu.VMEM) for a in (layer_out, new_state, window)]
+    layer_out, new_state, window = pl.pallas_call(
+        deliver_kernel,
+        out_shape=results,
+        in_specs=[vm] * 3,
+        out_specs=(hbm,) * 3,
+        scratch_shapes=[pltpu.SemaphoreType.DMA((3,))],
+        name="deliver",
+    )(*held)
     return (layer_out, new_state, window.transpose(1, 0, 2))
 
 

time: 83.7 us -> 80.1 us (0.957)
  local copies, waits for them, and re-layouts: 2.04 us -> 0 us
  Pallas kernels: 80.9 us -> 79.3 us
    pallas_call x1, Pallas kernels: 80.9 us -> 78.5 us  [in_kernel(): pl.pallas_call(functools.partial(layer_kernel, n, m, experts), out_shape=...]
    unnamed x3 -> x0, local copies, waits for them, and re-layouts: 2.04 us -> none
where the time goes in v3:
time: 80.1 us; the launch traced here: 80 us
  Pallas kernels  79.3 us (99%)
    pallas_call x1, Pallas kernels, in_kernel(): pl.pallas_call(functools.partial(layer_kernel, n, m, experts), out_shape=...  78.5 us

profile of v3, /device:TPU:0, one launch (start us, length us, event | category | flops | bytes accessed | tf_op | source)
XLA Modules:
  0.0 80.0 jit_solution(2422340010054244354)
XLA Ops:
  0.6 78.5 %layer.1 = (bf16[32,4096]{1,0:T(8,128)(2,1)S(1)}, f32[32,1024]{1,0:T(8,128)S(1)}, bf16[3,32,1024]{2,1,0:T(8,128)(2,1)S(1)}) custom-call(bf16[32,4096]{1,0:T(8,128)(2,1)} %tok_hbm.1, f32[8,1,512]{2,1,0:T(1,128)} %bitcast.15, f32[8,1,512]{2,1,0:T(1,128)} %bitcast.16, s32[2,32]{1,0:T(2,128)} %bitcast.18, f32[32,1024]{1,0:T(8,128)} %st_hbm.1, ...), custom_call_target="tpu_custom_call" | custom-call | tf_op jit(solution)/shard_map/layer/pallas_call | solution.py:826
  79.1 0.8 %deliver.1 = (bf16[32,4096]{1,0:T(8,128)(2,1)}, f32[32,1024]{1,0:T(8,128)}, bf16[3,32,1024]{2,1,0:T(8,128)(2,1)}) custom-call(bf16[32,4096]{1,0:T(8,128)(2,1)S(1)} %get-tuple-element.9.a, f32[32,1024]{1,0:T(8,128)S(1)} %get-tuple-element.10.b, bf16[3,32,1024]{2,1,0:T(8,128)(2,1)S(1)} %get-tuple-element.11.c), custom_call_target="tpu_custom_call" | custom-call | tf_op jit(solution)/shard_map/deliver/pallas_call | solution.py:866

commit v4 on v3

--- a/solution.py
+++ b/solution.py
@@ -248,11 +248,11 @@
     with jax.named_scope('greet'):
         pl.semaphore_wait(barrier, len(peers))
 
-    send(toks.at[:, lanes(mate, q)], narr.at[me], tr.at[me], mate, tp)
+    send(toks.at[:, lanes(mate, q)], narr.at[me], tr.at[0], mate, tp)
     for k in (2, 1, 3):
         for core in range(2):
             to = 2 * zp(k) + core
-            send(toks.at[:, lanes(to, q)], narr.at[me], tr.at[me], to, tp)
+            send(toks.at[:, lanes(to, q)], narr.at[me], tr.at[k], to, tp)
     narr[me] = toks[:, lanes(me, q)]
     lrt.wait()
     pair = jnp.concatenate([rts[...]] * zs, axis=1)
@@ -332,10 +332,7 @@
 
     def part(k):
         zz = zp(k)
-        for core in range(2):
-            slot = 2 * zz + (1 - c if core == 0 else c)
-            if k or core == 0:
-                arrive(narr.at[slot], tr.at[slot])
+        arrive(narr.at[pl.ds(2 * zz, 2)] if k else narr.at[mate], tr.at[k])
         x = jnp.concatenate([narr[2 * zz + 1 - c], narr[2 * zz + c]], axis=0)
         x = (x.astype(F32) * mgain[me]).astype(BF16)
         return jnp.concatenate([dot(x, iw[...]), dot(x, gw[...])], axis=1)
@@ -347,7 +344,8 @@
         first(0)
         lbig = [load(a, b) for a, b in ((ow_hbm, ow), (dg_hbm, dg), (du_hbm, du), (dd_hbm, dd))]
         lexp = [load(eg, wg), load(eu, wu)]
-        ldown = [load(ed.at[:, pl.ds(i * q, q)], wd.at[i]) for i in range(n)]
+        for i in range(n):
+            pltpu.make_async_copy(ed.at[:, pl.ds(i * q, q)], wd.at[i], lw.at[lw.shape[0] - 1]).start()
         for k in (2, 1):
             first(k)
             second(k)
@@ -412,25 +410,24 @@
         def pass_on(k):
             slot = 2 * zp(k) + c
             arrive(mall.at[slot], ar.at[k])
-            send(mall.at[slot], mall.at[slot], br.at[k], mate, tp)
+            send(mall.at[slot], mall.at[slot], br.at[k // 2], mate, tp)
 
         def mixed(i):
-            for k in (2 * i, 2 * i + 1):
-                arrive(mall.at[2 * zp(k) + 1 - c], br.at[k])
+            arrive(mall.at[pl.ds(0, 2)], br.at[i])
             which = side if i == 0 else 1 - side
             x = mall[pl.ds(which * zs, zs)].reshape(half, ch)
             y = dot(x, ow[...]).astype(BF16)
             for t in range(m):
                 osend[t, i] = y[:, t * g : (t + 1) * g]
             for k in (3, 1, 2):
-                send(osend.at[tx(k), i], orecv.at[k, i], or_.at[k, i], me, tx(k))
+                send(osend.at[tx(k), i], orecv.at[k, i], or_.at[i], me, tx(k))
 
         def summed(i):
             which = side if i == 0 else 1 - side
             raw = narr[pl.ds(which * zs, zs), :, lanes(tp, g)].reshape(half, g)
             total = raw.astype(F32) + osend[tp, i].astype(F32)
+            arrive(orecv.at[pl.ds(1, m - 1), i], or_.at[i])
             for k in range(1, m):
-                arrive(orecv.at[k, i], or_.at[k, i])
                 total += orecv[k, i].astype(F32)
             full[tp, me, which] = total.astype(BF16)
 
@@ -443,8 +440,8 @@
         slot, s = 2 * zp(k) + c, sided(k, i)
         at = full.at[tp, slot, s]
         for d in (3, 1, 2) if (k, i) in direct else (1, 2):
-            send(at, at, xr.at[d, k, s], me, tx(d))
-        send(at, at, mrv.at[0, k, s], mate, tp)
+            send(at, at, xr.at[d - 1, k, s], me, tx(d))
+        send(at, at, mrv.at[k, s], mate, tp)
 
     def own(i):
         at = full.at[tp, me, sided(0, i)]
@@ -463,19 +460,19 @@
         early = tx(1) * (1 - s) + tx(2) * s
         late = tx(2) * (1 - s) + tx(1) * s
         at = full.at[early, slot, s]
-        arrive(at, xr.at[1 + s, k, s])
+        arrive(at, xr.at[s, k, s])
         if (k, i) not in direct:
-            send(at, at, xr.at[3, k, s], me, late)
-        send(at, at, mrv.at[1 + s, k, s], mate, tp)
+            send(at, at, xr.at[2, k, s], me, late)
+        send(at, at, mrv.at[k, s], mate, tp)
         at = full.at[late, slot, s]
-        arrive(at, xr.at[2 - s, k, s])
-        send(at, at, mrv.at[2 - s, k, s], mate, tp)
+        arrive(at, xr.at[1 - s, k, s])
+        send(at, at, mrv.at[k, s], mate, tp)
 
     def relay_far(k, i):
         slot, s = 2 * zp(k) + c, sided(k, i)
         at = full.at[tx(3), slot, s]
-        arrive(at, xr.at[3, k, s])
-        send(at, at, mrv.at[3, k, s], mate, tp)
+        arrive(at, xr.at[2, k, s])
+        send(at, at, mrv.at[k, s], mate, tp)
 
     def absorb(e, s, keep):
         parts = []
@@ -498,8 +495,7 @@
 
     def absorb_mate(k, i):
         e, s = 2 * zp(k) + 1 - c, sided(k, i)
-        for d in range(m):
-            arrive(full.at[tx(d), e, s], mrv.at[d, k, s])
+        arrive(full.at[:, e, s], mrv.at[k, s])
         absorb(e, s, False)
 
     def dpart(k):
@@ -522,7 +518,7 @@
             for core in range(2):
                 if k or core:
                     to = 2 * zp(k) + (c if core == 0 else 1 - c)
-                    send(mask, masks.at[me], kr.at[me], to, tp)
+                    send(mask, masks.at[me], kr.at[0], to, tp)
         masks[me] = mask[...]
     with jax.named_scope("mix_sum"):
         pass_on(2)
@@ -545,39 +541,39 @@
         absorb_own(0, 0)
         dfirst(0)
         relay(3, 0)
+        absorb_mate(0, 0)
         relay_far(1, 0)
         dfirst(1)
-        absorb_own(1, 0)
-        absorb_mate(0, 0)
         relay(0, 1)
         relay_far(0, 1)
+        landed(1, 1)
         absorb_own(0, 1)
         dfirst(2)
+        landed(2, 1)
+        landed(3, 1)
         dsecond(1)
         dfirst(3)
-        landed(1, 1)
         relay_far(2, 0)
         dsecond(2)
         dlast_outer()
+        absorb_own(1, 0)
+        absorb_mate(1, 0)
+        relay(1, 1)
         absorb_own(2, 0)
-        absorb_mate(1, 0)
-        landed(2, 1)
-        landed(3, 1)
-        relay(1, 1)
         relay_far(3, 0)
+        relay(2, 1)
+        absorb_mate(2, 0)
+        relay_far(1, 1)
         absorb_own(3, 0)
-        absorb_mate(2, 0)
-        relay(2, 1)
+        relay(3, 1)
+        relay_far(2, 1)
         absorb_mate(3, 0)
-        relay_far(1, 1)
+        relay_far(3, 1)
+        dlast_inner()
         absorb_own(1, 1)
-        relay(3, 1)
-        dlast_inner()
         absorb_mate(0, 1)
-        relay_far(2, 1)
         absorb_own(2, 1)
         absorb_mate(1, 1)
-        relay_far(3, 1)
         absorb_own(3, 1)
         absorb_mate(2, 1)
         dsecond(0)
@@ -598,11 +594,7 @@
             send(dact, dall.at[me], cr.at[k], 2 * zp(k) + c, tp)
         send(dact, dall.at[me], er.at[0], mate, tp)
         dall[me] = dact[...]
-        for k in range(zs):
-            for core in range(2):
-                if k or core:
-                    src = 2 * zp(k) + (c if core == 0 else 1 - c)
-                    arrive(masks.at[src], kr.at[src])
+        arrive(masks.at[pl.ds(0, n - 1)], kr.at[0])
     weight, branch = [], []
 
     def activate(ih):
@@ -633,11 +625,11 @@
     joined = [(i, 1) for i in range(m - 1)]
 
     def pass_part(k, i, ih, part, to):
-        send(part, xrecv.at[k, i, ih], hr.at[k, i, ih], me, tx(to))
+        send(part, xrecv.at[k, i, ih], hr.at[1 if k == 3 and (i, ih) in joined else 0, i, ih], me, tx(to))
 
     def join(i, ih):
         lead = 1 + (i + ih) % 2
-        arrive(xrecv.at[3, i, ih], hr.at[3, i, ih])
+        arrive(xrecv.at[3, i, ih], hr.at[1, i, ih])
         total = kq[i, ih, tx(3 - lead)] + xrecv[3, i, ih].astype(F32)
         xjoin[i, ih] = total.astype(BF16)
         pass_part(3 - lead, i, ih, xjoin.at[i, ih], 3 - lead)
@@ -661,18 +653,18 @@
 
     def settle(i, ih):
         total = kq[i, ih, tp]
+        many = 2 if (i, ih) in joined else m - 1
+        arrive(xrecv.at[pl.ds(1, many), i, ih], hr.at[0, i, ih])
         for k in (1, 2) if (i, ih) in joined else range(1, m):
-            arrive(xrecv.at[k, i, ih], hr.at[k, i, ih])
             total += xrecv[k, i, ih].astype(F32)
         pbuf[i, ih] = total.reshape(2, 2 * rows, g)
         for k in (2, 3) if ih == 0 else (1,):
             zsend[k, i] = pbuf[i, ih, lax.rem(zp(k), 2)].astype(BF16)
 
     def away(k, i):
-        send(zsend.at[k, i], zrecv.at[k, i], gr.at[k, i], 2 * zp(k) + c, tp)
-
-    for cp in ldown:
-        cp.wait()
+        send(zsend.at[k, i], zrecv.at[k, i], gr.at[0], 2 * zp(k) + c, tp)
+
+    pltpu.make_async_copy(wd, wd, lw.at[lw.shape[0] - 1]).wait()
     with jax.named_scope("down_far"):
         activate(0)
         down(0)
@@ -681,11 +673,10 @@
         for k in (1, 2, 3):
             slot = 2 * zp(k) + c
             arrive(dall.at[slot], cr.at[k])
-            send(dall.at[slot], dall.at[slot], er.at[k], mate, tp)
+            send(dall.at[slot], dall.at[slot], er.at[0], mate, tp)
 
     def dense_ready():
-        for k in range(zs):
-            arrive(dall.at[2 * zp(k) + 1 - c], er.at[k])
+        arrive(dall.at[pl.ds(0, zs)], er.at[0])
 
     def dense_forward(ih):
         s = 1 - side if ih == 0 else side
@@ -744,9 +735,7 @@
             leave(3, 1)
 
     with jax.named_scope("last_sum"):
-        for k in range(1, zs):
-            for i in range(m):
-                arrive(zrecv.at[k, i], gr.at[k, i])
+        arrive(zrecv.at[pl.ds(1, zs - 1)], gr.at[0])
         spot = lax.rem(z, 2)
         for j in range(m):
             total = pbuf[lax.rem(j - z - 1 + 2 * m, m), 1, spot]
@@ -762,19 +751,15 @@
                 if k or dc:
                     core = c if dc == 0 else 1 - c
                     send(
-                        fblk.at[core], fin.at[c, tp], fr.at[dc, k], 2 * z + core, tx(k)
+                        fblk.at[core], fin.at[c * m + tp], fr.at[0], 2 * z + core, tx(k)
                     )
-        fin[c, tp] = fblk[c]
-        for k in (0, 1, 2, 3):
-            for dc in range(2):
-                if k or dc:
-                    core = c if dc == 0 else 1 - c
-                    arrive(fin.at[core, tx(k)], fr.at[dc, k])
+        fin[c * m + tp] = fblk[c]
+        arrive(fin.at[pl.ds(0, 2 * m - 1)], fr.at[0])
         for core in range(2):
             for t in range(m):
                 for j in range(m):
                     base = (2 * j + core) * q + t * g
-                    out[:, base : base + g] = fin[core, t, j]
+                    out[:, base : base + g] = fin[core * m + t, j]
     with jax.named_scope("drain"):
         for cp in sends:
             cp.wait_send()
@@ -851,11 +836,11 @@
             v((m, 2, m, half, g), BF16), v((m, m, 2, half, g), BF16), v((m - 1, 2, half, g), BF16),
             v((m, 2, 2, 2 * rows, g), F32),
             v((zs, m, 2 * rows, g), BF16), v((zs, m, 2 * rows, g), BF16),
-            v((2, m, rows, g), BF16), v((2, m, m, rows, g), BF16),
+            v((2, m, rows, g), BF16), v((2 * m, m, rows, g), BF16),
         ]
         + flags(
-            (32,), (1,), (n,), (n,), (zs,), (zs,), (zs,), (zs,), (m, 2), (zs, 2), (m, zs, 2), (m, zs, 2),
-            (zs,), (zs,), (zs,), (zs,), (m, 2), (m, m, 2), (zs, m), (2, m),
+            (21,), (1,), (zs,), (1,), (zs,), (zs,), (zs,), (2,), (2,), (zs, 2), (m - 1, zs, 2), (zs, 2),
+            (zs,), (zs,), (zs,), (1,), (m, 2), (2, m, 2), (1,), (1,),
         ),
         compiler_params=pltpu.CompilerParams(
             collective_id=0, has_side_effects=True, vmem_limit_bytes=58 * 1024 * 1024

time: 80.1 us -> 78.6 us (0.981)
  Pallas kernels: 79.3 us -> 77.8 us
    pallas_call x1, Pallas kernels: 78.5 us -> 77 us  [in_kernel(): pl.pallas_call(functools.partial(layer_kernel, n, m, experts), out_shape=...]
where the time goes in v4:
time: 78.6 us; the launch traced here: 78.5 us
  Pallas kernels  77.8 us (99%)
    pallas_call x1, Pallas kernels, in_kernel(): pl.pallas_call(functools.partial(layer_kernel, n, m, experts), out_shape=...  77 us

profile of v4, /device:TPU:0, one launch (start us, length us, event | category | flops | bytes accessed | tf_op | source)
XLA Modules:
  0.0 78.5 jit_solution(8174990991610407390)
XLA Ops:
  0.6 77.0 %layer.1 = (bf16[32,4096]{1,0:T(8,128)(2,1)S(1)}, f32[32,1024]{1,0:T(8,128)S(1)}, bf16[3,32,1024]{2,1,0:T(8,128)(2,1)S(1)}) custom-call(bf16[32,4096]{1,0:T(8,128)(2,1)} %tok_hbm.1, f32[8,1,512]{2,1,0:T(1,128)} %bitcast.15, f32[8,1,512]{2,1,0:T(1,128)} %bitcast.16, s32[2,32]{1,0:T(2,128)} %bitcast.18, f32[32,1024]{1,0:T(8,128)} %st_hbm.1, ...), custom_call_target="tpu_custom_call" | custom-call | tf_op jit(solution)/shard_map/layer/pallas_call | solution.py:811
  77.7 0.8 %deliver.1 = (bf16[32,4096]{1,0:T(8,128)(2,1)}, f32[32,1024]{1,0:T(8,128)}, bf16[3,32,1024]{2,1,0:T(8,128)(2,1)}) custom-call(bf16[32,4096]{1,0:T(8,128)(2,1)S(1)} %get-tuple-element.9.a, f32[32,1024]{1,0:T(8,128)S(1)} %get-tuple-element.10.b, bf16[3,32,1024]{2,1,0:T(8,128)(2,1)S(1)} %get-tuple-element.11.c), custom_call_target="tpu_custom_call" | custom-call | tf_op jit(solution)/shard_map/deliver/pallas_call | solution.py:851

commit v5 on v4

--- a/solution.py
+++ b/solution.py
@@ -401,7 +401,7 @@
 
     with jax.named_scope("mix"):
         send(mr, mall.at[me], br.at[0], mate, tp)
-        for k in range(1, zs):
+        for k in (1, 3, 2):
             send(mr, mall.at[me], ar.at[k], 2 * zp(k) + c, tp)
         mall[me] = mr[...]
         for cp in lbig:
@@ -431,7 +431,7 @@
                 total += orecv[k, i].astype(F32)
             full[tp, me, which] = total.astype(BF16)
 
-    direct = [(k, 1) for k in range(zs)]
+    direct = [(k, 1) for k in range(zs)] + [(0, 0)]
 
     def sided(k, i):
         return side if (k < 2) == (i == 0) else 1 - side

time: 78.6 us -> 76.4 us (0.972)
  Pallas kernels: 77.8 us -> 75.6 us
    pallas_call x1, Pallas kernels: 77 us -> 74.7 us  [in_kernel(): pl.pallas_call(functools.partial(layer_kernel, n, m, experts), out_shape=...]
where the time goes in v5:
time: 76.4 us; the launch traced here: 76.2 us
  Pallas kernels  75.6 us (99%)
    pallas_call x1, Pallas kernels, in_kernel(): pl.pallas_call(functools.partial(layer_kernel, n, m, experts), out_shape=...  74.7 us

profile of v5, /device:TPU:0, one launch (start us, length us, event | category | flops | bytes accessed | tf_op | source)
XLA Modules:
  0.0 76.2 jit_solution(7626508368070278400)
XLA Ops:
  0.6 74.7 %layer.1 = (bf16[32,4096]{1,0:T(8,128)(2,1)S(1)}, f32[32,1024]{1,0:T(8,128)S(1)}, bf16[3,32,1024]{2,1,0:T(8,128)(2,1)S(1)}) custom-call(bf16[32,4096]{1,0:T(8,128)(2,1)} %tok_hbm.1, f32[8,1,512]{2,1,0:T(1,128)} %bitcast.15, f32[8,1,512]{2,1,0:T(1,128)} %bitcast.16, s32[2,32]{1,0:T(2,128)} %bitcast.18, f32[32,1024]{1,0:T(8,128)} %st_hbm.1, ...), custom_call_target="tpu_custom_call" | custom-call | tf_op jit(solution)/shard_map/layer/pallas_call | solution.py:811
  75.4 0.8 %deliver.1 = (bf16[32,4096]{1,0:T(8,128)(2,1)}, f32[32,1024]{1,0:T(8,128)}, bf16[3,32,1024]{2,1,0:T(8,128)(2,1)}) custom-call(bf16[32,4096]{1,0:T(8,128)(2,1)S(1)} %get-tuple-element.9.a, f32[32,1024]{1,0:T(8,128)S(1)} %get-tuple-element.10.b, bf16[3,32,1024]{2,1,0:T(8,128)(2,1)S(1)} %get-tuple-element.11.c), custom_call_target="tpu_custom_call" | custom-call | tf_op jit(solution)/shard_map/deliver/pallas_call | solution.py:851
